TPU v7x, 512 devices: a whole 4x8x8 slice. The times are simulated.
512 devices in a mesh: ep: 128 (over z, y, core), tp: 4 (over x).
Axes of the slice: x: 4, y: 8, z: 8, core: 2. Of those that a mesh axis runs over, the one named last changes fastest.
Arguments:
- tokens: bfloat16 [2048, 1024], P('ep', 'tp'), may hold values from -12 to 12
- input_window: bfloat16 [2048, 3, 512], P('ep', None, 'tp'), may hold values from -6 to 6
- write_window: bfloat16 [2048, 3, 256], P('ep', None, 'tp'), may hold values from -6 to 6
- read_window: bfloat16 [2048, 3, 256], P('ep', None, 'tp'), may hold values from -6 to 6
- ssm_state: float32 [2048, 8, 64, 64], P('ep', 'tp'), may hold values from -6 to 6
- norm_gain: bfloat16 [1024], replicated, may hold values from 0.099609375 to 1.8984375
- proj_gate: bfloat16 [1024, 512], P(None, 'tp'), may hold values from -0.1875 to 0.1875
- proj_input: bfloat16 [1024, 512], P(None, 'tp'), may hold values from -0.1875 to 0.1875
- proj_write: bfloat16 [1024, 256], P(None, 'tp'), may hold values from -0.1875 to 0.1875
- proj_read: bfloat16 [1024, 256], P(None, 'tp'), may hold values from -0.1875 to 0.1875
- proj_step: bfloat16 [1024, 8], replicated, may hold values from -0.1875 to 0.1875
- taps_input: bfloat16 [4, 512], P(None, 'tp'), may hold values from -3 to 3
- taps_write: bfloat16 [4, 256], P(None, 'tp'), may hold values from -3 to 3
- taps_read: bfloat16 [4, 256], P(None, 'tp'), may hold values from -3 to 3
- step_bias: float32 [8], replicated, may hold values from -2.5 to 0.5
- decay_rate: float32 [8], replicated, may hold values from 0.02 to 2
- skip_gain: float32 [8], replicated, may hold values from 0.1 to 1.9
- out_gain: bfloat16 [512], P('tp'), may hold values from 0.099609375 to 1.8984375
- proj_out: bfloat16 [512, 1024], P('tp'), may hold values from -0.25 to 0.25
- ffn_gain: bfloat16 [1024], replicated, may hold values from 0.099609375 to 1.8984375
- expert_ids: int32 [2048, 6], P('ep'), may hold values from 0 to 127, all different within a row; in each aligned block of 16 rows (0 to 15, 16 to 31, ...) at most 2 rows name the same one
- expert_weights: float32 [2048, 6], P('ep'), may hold values from 0.05 to 1
- expert_gate: bfloat16 [128, 1024, 512], P('ep', None, 'tp'), may hold values from -0.1875 to 0.1875
- expert_up: bfloat16 [128, 1024, 512], P('ep', None, 'tp'), may hold values from -0.1875 to 0.1875
- expert_down: bfloat16 [128, 512, 1024], P('ep', 'tp'), may hold values from -0.25 to 0.25
- dense_gate: bfloat16 [1024, 1024], P(None, 'tp'), may hold values from -0.1875 to 0.1875
- dense_up: bfloat16 [1024, 1024], P(None, 'tp'), may hold values from -0.1875 to 0.1875
- dense_down: bfloat16 [1024, 1024], P(None, 'tp'), may hold values from -0.5 to 0.5
- branch_gate: bfloat16 [1024], replicated, may hold values from -0.1875 to 0.1875
Outputs:
- new_hidden: bfloat16 [2048, 1024], P('ep', 'tp')
- new_state: float32 [2048, 8, 64, 64], P('ep', 'tp')
- new_input_window: bfloat16 [2048, 3, 512], P('ep', None, 'tp')
- new_write_window: bfloat16 [2048, 3, 256], P('ep', None, 'tp')
- new_read_window: bfloat16 [2048, 3, 256], P('ep', None, 'tp')
Inputs may be any that keep to these rules, and one draw needn't show every extreme that they name: `expert_ids`: each row names 6 different experts. Among the 16 rows of one index of ep no expert is named more than 2 times, and in some aligned block an expert is named exactly 2 times.
All inputs are finite; a program needn't handle non-finite values.
Results may differ from a plain program's by a relative error of at most 0.018.
Values may be sent and summed in bfloat16 or wider, within the bound.
No kernel may reach another device: no remote copies, remote signals or barrier semaphores. Data moves between devices by JAX's collectives and lax.ppermute only.
A program may use at most 64 MiB of HBM per device.

v0:
```python
import jax
import jax.numpy as jnp
from jax import lax
from jax.experimental import pallas as pl
from jax.experimental.pallas import tpu as pltpu
from jax.sharding import PartitionSpec as P


HEADS = 8
HEAD_DIM = 64
STATE = 64
EPS = 1e-06
F32 = jnp.float32
BF16 = jnp.bfloat16

HBM = pl.BlockSpec(memory_space=pltpu.HBM)
VMEM = pl.BlockSpec(memory_space=pltpu.VMEM)
SMEM = pl.BlockSpec(memory_space=pltpu.SMEM)
INTERPRET = False
LIMIT = 16 * 1024 * 1024


def call(body, outs, specs, scratch=(), out_spec=VMEM):
    return pl.pallas_call(
        body,
        out_shape=outs,
        in_specs=specs,
        out_specs=out_spec
        if isinstance(out_spec, tuple)
        else jax.tree.map(lambda _: out_spec, outs),
        scratch_shapes=scratch,
        compiler_params=pltpu.CompilerParams(vmem_limit_bytes=LIMIT),
        interpret=INTERPRET,
    )


def kept(value):
    return pltpu.with_memory_space_constraint(value, pltpu.HBM)


def sds(shape, dtype):
    return jax.ShapeDtypeStruct(shape, dtype)


def nt(a, b):
    return lax.dot_general(a, b, (((1,), (1,)), ((), ())), preferred_element_type=F32)


def nn(a, b):
    return jnp.dot(a, b, preferred_element_type=F32)


def silu(v):
    return v / (1.0 + jnp.exp(-v))


def softplus(v):
    return jnp.maximum(v, 0.0) + jnp.log1p(jnp.exp(-jnp.abs(v)))


def spread_body(tokens, out, here, sems):
    first = pltpu.make_async_copy(tokens, here, sems.at[out.shape[0]])
    first.start()
    first.wait()
    copies = [pltpu.make_async_copy(here, out.at[j], sems.at[j]) for j in range(out.shape[0])]
    for copy in copies:
        copy.start()
    for copy in copies:
        copy.wait()


def zeros_and_ones(shape, test):
    across = lax.broadcasted_iota(jnp.int32, shape, 1)
    down = lax.broadcasted_iota(jnp.int32, shape, 0)
    return test(down, across).astype(F32).astype(BF16)


def route_body(rank, ids_there, weights_there, select, combine, ids, weights, sems):
    copies = [
        pltpu.make_async_copy(ids_there, ids, sems.at[0]),
        pltpu.make_async_copy(weights_there, weights, sems.at[1]),
    ]
    for copy in copies:
        copy.start()
    for copy in copies:
        copy.wait()
    tops, rows = ids.shape
    experts = combine.shape[1] // 8
    pieces = select.shape[0] // experts
    expert = lax.broadcasted_iota(jnp.int32, (experts, rows), 0)
    hits = jnp.zeros((experts, rows), F32)
    amount = jnp.zeros((experts, rows), F32)
    for k in range(tops):
        same = expert == ids[k : k + 1, :]
        hits = jnp.where(same, 1.0, hits)
        amount = jnp.where(same, weights[k : k + 1, :], amount)
    earlier = zeros_and_ones((rows, rows), lambda d, a: d < a)
    place = nn(hits.astype(BF16), earlier)
    mine = jnp.bitwise_and(rank[0], 1).astype(F32)
    chosen = jnp.where(place == mine, hits, 0.0).astype(BF16)
    down = zeros_and_ones((experts * pieces, experts), lambda d, a: d // pieces == a)
    across = zeros_and_ones((rows, rows * pieces), lambda d, a: a // pieces == d)
    wide = nn(nn(down, chosen).astype(BF16), across)
    matched = zeros_and_ones(wide.shape, lambda d, a: d % pieces == a % pieces)
    select[...] = wide.astype(BF16) * matched
    twice = zeros_and_ones((experts, experts * 2), lambda d, a: a // 2 == d)
    halves = lax.broadcasted_iota(jnp.int32, (rows, experts * 2), 1) % 2
    for s in range(2):
        part = jnp.where(place == float(s), amount, 0.0).T
        high = part.astype(BF16)
        low = (part - high.astype(F32)).astype(BF16)
        for p, piece in enumerate((high, low)):
            both = nn(piece, twice)
            for h in range(2):
                rows_at = (2 * p + h) * rows
                kept = jnp.where(halves == h, both, 0.0).astype(BF16)
                for t in (s, s + 2):
                    combine[
                        rows_at : rows_at + rows, t * 2 * experts : (t + 1) * 2 * experts
                    ] = kept


STAGED = 9


def prepare_body(*refs):
    rank, bias, rate, skip, gate, up, down = refs[:7]
    proj_gate, proj_input, proj_write, proj_read, proj_step = refs[7:12]
    sources = refs[12 : 12 + STAGED]
    lanes, packed, across, along = refs[12 + STAGED : 16 + STAGED]
    targets = refs[16 + STAGED : 16 + 2 * STAGED]
    bias_here, rate_here, skip_here, built, sems = refs[16 + 2 * STAGED :]
    width, block = gate.shape
    inner = proj_gate.shape[1]
    latent = proj_write.shape[0]
    pairs = [
        (bias, bias_here),
        (rate, rate_here),
        (skip, skip_here),
    ]
    pairs += [(gate, built.at[0:width]), (up, built.at[width : 2 * width])]
    for j in range(width // block):
        first = 2 * width + j * block
        pairs.append((down.at[:, j * block : (j + 1) * block], built.at[first : first + block]))
    building = len(pairs)
    pairs += [
        (proj_gate, across.at[:, 0:inner]),
        (proj_input, across.at[:, inner : 2 * inner]),
        (proj_write, along.at[0:latent]),
        (proj_read, along.at[latent : 2 * latent]),
        (proj_step, along.at[2 * latent : 2 * latent + HEADS]),
    ]
    pairs += list(zip(sources, targets))
    copies = [pltpu.make_async_copy(a, b, sems.at[k]) for k, (a, b) in enumerate(pairs)]
    out_copy = pltpu.make_async_copy(built, packed, sems.at[len(pairs)])
    for copy in copies:
        copy.start()
    for copy in copies[:building]:
        copy.wait()
    out_copy.start()
    heads = inner // HEAD_DIM
    lane_head = lax.broadcasted_iota(jnp.int32, (1, inner), 1) // HEAD_DIM
    for k, table in enumerate((bias_here, rate_here, skip_here)):
        line = jnp.zeros((1, inner), F32)
        for h in range(heads):
            line = jnp.where(lane_head == h, table[rank[0] * heads + h], line)
        lanes[k : k + 1, :] = line
    for copy in copies[building:]:
        copy.wait()
    out_copy.wait()


def conv(window, newest, taps, out_window):
    taken = taps[...].astype(F32)
    total = newest.astype(F32) * taken[3:4]
    for k in range(3):
        total += window[k].astype(F32) * taken[k : k + 1]
    out_window[0] = window[1]
    out_window[1] = window[2]
    out_window[2] = newest
    return silu(total)


def mixer_body(
    rank,
    lanes,
    arrived,
    across,
    along,
    norm_gain,
    taps_input,
    taps_write,
    taps_read,
    input_window,
    write_window,
    read_window,
    state,
    out_gain,
    proj_out,
    partial,
    new_state,
    new_input_window,
    new_write_window,
    new_read_window,
):
    rows = arrived.shape[1]
    x = jnp.concatenate([arrived[j] for j in range(arrived.shape[0])], axis=1).astype(F32)
    scale = lax.rsqrt(jnp.mean(x * x, axis=-1, keepdims=True) + EPS)
    normed = (x * scale * norm_gain[...].astype(F32)[None, :]).astype(BF16)
    inner = input_window.shape[2]
    latent = write_window.shape[2]
    first = nn(normed, across[...])
    second = nt(normed, along[...])
    gate_rows = first[:, 0:inner].astype(BF16)
    input_rows = first[:, inner : 2 * inner].astype(BF16)
    write_rows = second[:, 0:latent].astype(BF16)
    read_rows = second[:, latent : 2 * latent].astype(BF16)
    step_all = second[:, 2 * latent : 2 * latent + HEADS]
    input_conv = conv(input_window, input_rows, taps_input, new_input_window)
    write_conv = conv(write_window, write_rows, taps_write, new_write_window)
    read_conv = conv(read_window, read_rows, taps_read, new_read_window)
    heads = inner // HEAD_DIM
    lane_head = lax.broadcasted_iota(jnp.int32, (rows, inner), 1) // HEAD_DIM
    column = lax.broadcasted_iota(jnp.int32, step_all.shape, 1)
    raw = jnp.zeros((rows, inner), F32)
    for h in range(heads):
        mine = column == rank[0] * heads + h
        raw = jnp.where(
            lane_head == h, jnp.sum(jnp.where(mine, step_all, 0.0), axis=1, keepdims=True), raw
        )
    step = softplus(raw + lanes[0:1, :])
    decay = jnp.exp(-step * lanes[1:2, :])
    scaled_t = (step * input_conv).T
    decay_t = decay.T
    lane = lax.broadcasted_iota(jnp.int32, (inner, rows), 1)
    readout_t = jnp.zeros((inner, rows), F32)
    for b in range(rows):
        fresh = (
            decay_t[:, b : b + 1] * state[b] + scaled_t[:, b : b + 1] * write_conv[b : b + 1, :]
        )
        new_state[b] = fresh
        seen = jnp.sum(fresh * read_conv[b : b + 1, :], axis=1, keepdims=True)
        readout_t = jnp.where(lane == b, seen, readout_t)
    readout = readout_t.T + lanes[2:3, :] * input_conv
    gated = readout * silu(gate_rows.astype(F32))
    gated = gated * lax.rsqrt(jnp.mean(gated * gated, axis=-1, keepdims=True) + EPS)
    mixer_rows = (gated * out_gain[...].astype(F32)[None, :]).astype(BF16)
    mixed = nn(mixer_rows, proj_out[...]).astype(BF16)
    for j in range(partial.shape[0]):
        partial[j] = mixed


def hidden_body(
    rank, arrived, mixed_in, ffn_gain, select, outgoing, normed_out, hidden_part, folded
):
    count, rows, quarter = arrived.shape
    x = jnp.concatenate([arrived[j] for j in range(count)], axis=1).astype(F32)
    mixed = mixed_in[0].astype(F32)
    for j in range(1, count):
        mixed += mixed_in[j].astype(F32)
    hidden = (x + mixed).astype(BF16)
    wide = hidden.astype(F32)
    scale = lax.rsqrt(jnp.mean(wide * wide, axis=-1, keepdims=True) + EPS)
    normed_wide = wide * scale * ffn_gain[...].astype(F32)[None, :]
    normed_out[...] = normed_wide.astype(BF16)
    pieces = folded.shape[0] // rows
    for j in range(pieces):
        folded[pl.ds(j, rows, stride=pieces), :] = normed_wide[:, j * 128 : (j + 1) * 128]
    outgoing[...] = nn(select[...], folded[...].astype(BF16)).astype(BF16)
    part = wide[:, 0:quarter]
    for j in range(1, count):
        part = jnp.where(rank[0] == j, wide[:, j * quarter : (j + 1) * quarter], part)
    hidden_part[...] = part.astype(BF16)


def dense_body(rank, normed_in, gate, up, down, branch_gate, give, keep, branch):
    normed = normed_in[...]
    hidden = (silu(nn(normed, gate[...])) * nn(normed, up[...])).astype(BF16)
    total = nt(hidden, down[...]).astype(BF16)
    half = give.shape[1]
    upper = rank[0] > 1
    give[...] = jnp.where(upper, total[:, 0:half], total[:, half:])
    keep[...] = jnp.where(upper, total[:, half:], total[:, 0:half])
    level = jnp.sum(
        normed.astype(F32) * branch_gate[...].astype(F32)[None, :], axis=-1, keepdims=True
    )
    branch[...] = jnp.broadcast_to(jax.nn.sigmoid(level), branch.shape)


def halve_body(rank, keep, got, give, left):
    total = keep[...].astype(F32) + got[...].astype(F32)
    quarter = give.shape[1]
    odd = jnp.bitwise_and(rank[0], 1) > 0
    give[...] = jnp.where(odd, total[:, 0:quarter], total[:, quarter:]).astype(BF16)
    left[...] = jnp.where(odd, total[:, quarter:], total[:, 0:quarter])


def expert_body(items, gate, up, down, other, out, unfolded, fold):
    width, block = gate.shape
    pieces = width // 128
    count = items.shape[0] // pieces
    unfolded[...] = items[...].astype(F32)
    x = jnp.concatenate(
        [unfolded[pl.ds(j, count, stride=pieces), :].astype(BF16) for j in range(pieces)], axis=1
    )
    act = (silu(nn(x, gate[...])) * nn(x, up[...])).astype(BF16)
    act_other = (silu(nn(x, other[0:width])) * nn(x, other[width : 2 * width])).astype(BF16)
    total = nn(act, down[...])
    for j in range(pieces):
        first = 2 * width + j * block
        piece = total[:, j * block : (j + 1) * block] + nn(act_other, other[first : first + block])
        fold[pl.ds(j // 2 * 2 * count + j % 2, count, stride=2), :] = piece
    out[...] = fold[...].astype(BF16)


def final_body(returned, combine, left, got, branch, hidden_part, out):
    total = hidden_part[...].astype(F32)
    rows = total.shape[0]
    dense = left[...] + got[...].astype(F32)
    sums = nn(combine[...], returned[...])
    sums = sums[0 : 2 * rows] + sums[2 * rows :]
    total += jnp.concatenate([sums[0:rows], sums[rows:]], axis=1)
    total += branch[:, 0:1] * dense
    out[...] = total.astype(BF16)


def local(
    tokens,
    input_window,
    write_window,
    read_window,
    ssm_state,
    norm_gain,
    proj_gate,
    proj_input,
    proj_write,
    proj_read,
    proj_step,
    taps_input,
    taps_write,
    taps_read,
    step_bias,
    decay_rate,
    skip_gain,
    out_gain,
    proj_out,
    ffn_gain,
    expert_ids,
    expert_weights,
    expert_gate,
    expert_up,
    expert_down,
    dense_gate,
    dense_up,
    dense_down,
    branch_gate,
):
    tps = lax.axis_size("tp")
    eps = lax.axis_size("ep")
    rank = lax.axis_index("tp").astype(jnp.int32).reshape(1)
    rows, quarter = tokens.shape
    width = quarter * tps
    inner = proj_gate.shape[1]
    latent = proj_write.shape[1]
    heads = ssm_state.shape[1]
    block = expert_gate.shape[2]

    pieces = width // 128

    spread = call(
        spread_body,
        sds((tps, rows, quarter), BF16),
        [HBM],
        [pltpu.VMEM((rows, quarter), BF16), pltpu.SemaphoreType.DMA((tps + 1,))],
        HBM,
    )(kept(tokens))
    arrived = lax.all_to_all(spread, "tp", 0, 0, tiled=True)

    projections = (proj_gate, proj_input, proj_write.T, proj_read.T, proj_step.T)
    staged = (
        norm_gain,
        taps_input,
        taps_write,
        taps_read,
        input_window.transpose(1, 0, 2),
        write_window.transpose(1, 0, 2),
        read_window.transpose(1, 0, 2),
        ssm_state.reshape(rows, inner, STATE),
        out_gain,
    )
    lanes, packed, *staged = call(
        prepare_body,
        (
            pltpu.VMEM((8, inner), F32),
            pltpu.HBM((3 * width, block), BF16),
            pltpu.VMEM((width, 2 * inner), BF16),
            pltpu.VMEM((2 * latent + HEADS, width), BF16),
        )
        + tuple(pltpu.VMEM(v.shape, v.dtype) for v in staged),
        [SMEM] + [HBM] * (11 + STAGED),
        [
            pltpu.SMEM(step_bias.shape, F32),
            pltpu.SMEM(step_bias.shape, F32),
            pltpu.SMEM(step_bias.shape, F32),
            pltpu.VMEM((3 * width, block), BF16),
            pltpu.SemaphoreType.DMA((11 + pieces + STAGED,)),
        ],
        (VMEM, HBM) + (VMEM,) * (2 + STAGED),
    )(
        rank,
        *map(
            kept,
            (
                step_bias,
                decay_rate,
                skip_gain,
                expert_gate[0],
                expert_up[0],
                expert_down[0],
                *projections,
                *staged,
            ),
        ),
    )

    partial, new_state, new_input, new_write, new_read = call(
        mixer_body,
        (
            pltpu.HBM((tps, rows, width), BF16),
            sds((rows, inner, STATE), F32),
            sds((3, rows, inner), BF16),
            sds((3, rows, latent), BF16),
            sds((3, rows, latent), BF16),
        ),
        [SMEM] + [VMEM] * 14,
    )(rank, lanes, arrived, *staged, proj_out)
    mixed_in = lax.all_to_all(partial, "tp", 0, 0, tiled=True)
    ids, weights = expert_ids.T, expert_weights.T
    packed, ids, weights, _ = lax.optimization_barrier((packed, ids, weights, partial))
    select, combine = call(
        route_body,
        (
            sds((eps * pieces, rows * pieces), BF16),
            sds((4 * rows, 2 * tps * eps), BF16),
        ),
        [SMEM, HBM, HBM],
        [
            pltpu.VMEM(ids.shape, ids.dtype),
            pltpu.VMEM(weights.shape, F32),
            pltpu.SemaphoreType.DMA((2,)),
        ],
    )(rank, kept(ids), kept(weights))
    other = lax.ppermute(packed, "tp", [(t, t ^ 1) for t in range(tps)])

    outgoing, normed_ffn, hidden_part = call(
        hidden_body,
        (
            pltpu.HBM((eps * pieces, 128), BF16),
            sds((rows, width), BF16),
            sds((rows, quarter), BF16),
        ),
        [SMEM] + [VMEM] * 4,
        [pltpu.VMEM((rows * pieces, 128), F32)],
    )(rank, arrived, mixed_in, ffn_gain, select)
    items = lax.all_to_all(outgoing.reshape(eps, pieces, 128), "ep", 0, 0, tiled=True)

    give, keep, branch = call(
        dense_body,
        (sds((rows, width // 2), BF16), sds((rows, width // 2), BF16), sds((rows, 128), F32)),
        [SMEM] + [VMEM] * 5,
    )(rank, normed_ffn, dense_gate, dense_up, dense_down, branch_gate)
    got = lax.ppermute(give, "tp", [(t, t ^ 2) for t in range(tps)])
    give, left = call(
        halve_body, (sds((rows, quarter), BF16), sds((rows, quarter), F32)), [SMEM] + [VMEM] * 2
    )(rank, keep, got)
    items, give = lax.optimization_barrier((items, give))
    got = lax.ppermute(give, "tp", [(t, t ^ 1) for t in range(tps)])

    results = call(
        expert_body,
        pltpu.HBM((tps * eps * 2, 128), BF16),
        [VMEM] * 5,
        [pltpu.VMEM((eps * pieces, 128), F32), pltpu.VMEM((tps * eps * 2, 128), F32)],
    )(items.reshape(eps * pieces, 128), expert_gate[0], expert_up[0], expert_down[0], other)
    returned = lax.all_to_all(
        results.reshape(tps * eps, 2, 128), ("tp", "ep"), 0, 0, tiled=True
    ).reshape(tps * eps * 2, 128)

    new_hidden = call(final_body, sds((rows, quarter), BF16), [VMEM] * 6)(
        returned, combine, left, got, branch, hidden_part
    )
    return (
        new_hidden,
        new_state.reshape(rows, heads, HEAD_DIM, STATE),
        new_input.transpose(1, 0, 2),
        new_write.transpose(1, 0, 2),
        new_read.transpose(1, 0, 2),
    )


def solution(mesh):
    in_specs = (
        P("ep", "tp"),
        P("ep", None, "tp"),
        P("ep", None, "tp"),
        P("ep", None, "tp"),
        P("ep", "tp", None, None),
        P(),
        P(None, "tp"),
        P(None, "tp"),
        P(None, "tp"),
        P(None, "tp"),
        P(),
        P(None, "tp"),
        P(None, "tp"),
        P(None, "tp"),
        P(),
        P(),
        P(),
        P("tp"),
        P("tp", None),
        P(),
        P("ep", None),
        P("ep", None),
        P("ep", None, "tp"),
        P("ep", None, "tp"),
        P("ep", "tp", None),
        P(None, "tp"),
        P(None, "tp"),
        P(None, "tp"),
        P(),
    )
    out_specs = (
        P("ep", "tp"),
        P("ep", "tp", None, None),
        P("ep", None, "tp"),
        P("ep", None, "tp"),
        P("ep", None, "tp"),
    )
    return jax.shard_map(local, mesh=mesh, in_specs=in_specs, out_specs=out_specs, check_vma=False)
```

profile of v0, /device:TPU:1, one launch (start us, length us, event | category | flops | bytes accessed | tf_op | source)
XLA Modules:
  0.0 99.9 jit_solution(8757922749715839868)
XLA Ops:
  0.6 1.3 %shard_map.308 = bf16[4,16,256]{2,1,0:T(8,128)(2,1)} custom-call(bf16[16,256]{1,0:T(8,128)(2,1)} %tokens.1), custom_call_target="tpu_custom_call" | custom-call | tf_op jit(solution)/shard_map/pallas_call | solution.py:370
  2.0 4.8 %all-to-all-start = ((bf16[4,16,256]{2,1,0:T(8,128)(2,1)}), bf16[4,16,256]{2,1,0:T(8,128)(2,1)S(1)}, u32[]{:S(2)}, u32[]{:S(2)}) async-start(bf16[4,16,256]{2,1,0:T(8,128)(2,1)} %shard_map.308), calls=%async_computation | async-start | bytes 65536 | tf_op jit(solution)/shard_map/all_to_all | solution.py:377
  6.8 0.0 copy-start.6
  6.8 2.2 %shard_map.309 = (f32[8,128]{1,0:T(8,128)S(1)}, bf16[3072,128]{1,0:T(8,128)(2,1)}, bf16[1024,256]{1,0:T(8,128)(2,1)S(1)}, bf16[136,1024]{1,0:T(8,128)(2,1)S(1)},...) custom-call(s32[1]{0:T(128)} %bitcast.refs_0_.rank, ...), custom_call_target="tpu_custom_call" | custom-call | tf_op jit(solution)/shard_map/pallas_call | solution.py:391
  9.1 2.1 %all-to-all-done.arrived = bf16[4,16,256]{2,1,0:T(8,128)(2,1)S(1)} async-done(((bf16[4,16,256]{2,1,0:T(8,128)(2,1)}), bf16[4,16,256]{2,1,0:T(8,128)(2,1)S(1)}, u32[]{:S(2)}, u32[]{:S(2)}) %all-to-all-start) | async-done | bytes 32800 | tf_op jit(solution)/shard_map/all_to_all | solution.py:377
  11.1 0.0 copy-done.6
  11.1 0.0 copy-start.9
  11.1 0.0 copy-start.5
  11.1 3.3 %shard_map.310 = (bf16[4,16,1024]{2,1,0:T(8,128)(2,1)}, f32[16,128,64]{2,1,0:T(8,128)}, bf16[3,16,128]{2,1,0:T(8,128)(2,1)}, bf16[3,16,64]{2,1,0:T(8,128)(2,1)}, bf16[3,16,64]{2,1,0:T(8,128)(2,1)}) custom-call(s32[1]{0:T(128)} %bitcast.refs_0_.rank, f32[8,128]{1,0:T(8,128)S(1)} %get-tuple-element.38.lanes, bf16[4,16,256]{2,1,0:T(8,128)(2,1)S(1)} %all-to-all-done.arrived, ...), custom_call_target="tpu_custom_call" | custom-call | tf_op jit(solution)/shard_map/pallas_call | solution.py:426
  14.4 2.2 %collective-permute-start.1 = (bf16[3072,128]{1,0:T(8,128)(2,1)}, bf16[3072,128]{1,0:T(8,128)(2,1)S(1)}, u32[]{:S(2)}, u32[]{:S(2)}) collective-permute-start(bf16[3072,128]{1,0:T(8,128)(2,1)} %get-tuple-element.61), channel_id=1, source_target_pairs={{0,1},{1,0},{2,3},{3,2},{4,5},{5,4},{6,7},{7,6},{8,9},{9,8},{10,11... | collective-permute-start | bytes 2359304 | tf_op jit(solution)/shard_map/ppermute | solution.py:453
  16.6 0.0 copy-start.4
  16.6 3.5 %all-to-all-start.1 = ((bf16[4,16,1024]{2,1,0:T(8,128)(2,1)}), bf16[4,16,1024]{2,1,0:T(8,128)(2,1)S(1)}, u32[]{:S(2)}, u32[]{:S(2)}) async-start(bf16[4,16,1024]{2,1,0:T(8,128)(2,1)} %get-tuple-element.50), calls=%async_computation.1 | async-start | bytes 262144 | tf_op jit(solution)/shard_map/all_to_all | solution.py:437
  20.1 0.0 copy-start.3
  20.1 1.4 %shard_map.311 = (bf16[1024,128]{1,0:T(8,128)(2,1)S(1)}, bf16[64,1024]{1,0:T(8,128)(2,1)S(1)}) custom-call(s32[1]{0:T(128)} %bitcast.refs_0_.rank, s32[6,16]{1,0:T(8,128)} %bitcast.38, f32[6,16]{1,0:T(8,128)} %bitcast.39), custom_call_target="tpu_custom_call" | custom-call | tf_op jit(solution)/shard_map/pallas_call | solution.py:440
  21.5 0.0 copy-start.7
  21.5 9.5 %all-to-all-done.1.mixed_in = bf16[4,16,1024]{2,1,0:T(8,128)(2,1)S(1)} async-done(((bf16[4,16,1024]{2,1,0:T(8,128)(2,1)}), bf16[4,16,1024]{2,1,0:T(8,128)(2,1)S(1)}, u32[]{:S(2)}, u32[]{:S(2)}) %all-to-all-start.1) | async-done | bytes 131104 | tf_op jit(solution)/shard_map/all_to_all | solution.py:437
  31.0 0.0 copy-done.9
  31.0 1.0 %shard_map.312 = (bf16[1024,128]{1,0:T(8,128)(2,1)}, bf16[16,1024]{1,0:T(8,128)(2,1)S(1)}, bf16[16,256]{1,0:T(8,128)(2,1)S(1)}) custom-call(s32[1]{0:T(128)} %bitcast.refs_0_.rank, bf16[4,16,256]{2,1,0:T(8,128)(2,1)S(1)} %all-to-all-done.arrived, bf16[4,16,1024]{2,1,0:T(8,128)(2,1)S(1)} %all-to-all-done.1.mixed_in, bf16[1024]{0:T(1024)(128)(2,1)S(1)} %copy-done.9, ...), custom_call_target="tpu_custom_call" | custom-call | tf_op jit(solution)/shard_map/pallas_call | solution.py:455
  32.0 0.0 copy-done.7
  32.0 0.0 copy-start.10
  32.0 24.6 %all-to-all-start.2 = ((bf16[128,8,128]{2,1,0:T(8,128)(2,1)}), bf16[128,8,128]{2,1,0:T(8,128)(2,1)S(1)}, u32[]{:S(2)}, u32[]{:S(2)}) async-start(bf16[128,8,128]{2,1,0:T(8,128)(2,1)} %bitcast.31), calls=%async_computation.2 | async-start | bytes 524288 | tf_op jit(solution)/shard_map/all_to_all | solution.py:465
  56.6 0.0 copy-done.5
  56.6 0.0 copy-done.4
  56.6 0.0 copy-done.3
  56.6 0.0 copy-done.10
  56.6 0.0 copy-start
  56.7 0.0 copy-start.1
  56.7 0.0 copy-start.2
  56.7 0.4 shard_map.313
  57.1 3.1 %collective-permute-start = (bf16[16,512]{1,0:T(8,128)(2,1)S(1)}, bf16[16,512]{1,0:T(8,128)(2,1)S(1)}, u32[]{:S(2)}, u32[]{:S(2)}) collective-permute-start(bf16[16,512]{1,0:T(8,128)(2,1)S(1)} %get-tuple-element.58), channel_id=1, source_target_pairs={{0,2},{1,3},{2,0},{3,1},{4,6},{5,7},{6,4},{7,5},{8,10},{9,11},{10,... | collective-permute-start | bytes 49160 | tf_op jit(solution)/shard_map/ppermute | solution.py:472
  60.2 3.2 %collective-permute-done.got = bf16[16,512]{1,0:T(8,128)(2,1)S(1)} collective-permute-done((bf16[16,512]{1,0:T(8,128)(2,1)S(1)}, bf16[16,512]{1,0:T(8,128)(2,1)S(1)}, u32[]{:S(2)}, u32[]{:S(2)}) %collective-permute-start) | collective-permute-done | bytes 16416 | tf_op jit(solution)/shard_map/ppermute | solution.py:472
  63.4 8.4 %all-to-all-done.2 = bf16[128,8,128]{2,1,0:T(8,128)(2,1)S(1)} async-done(((bf16[128,8,128]{2,1,0:T(8,128)(2,1)}), bf16[128,8,128]{2,1,0:T(8,128)(2,1)S(1)}, u32[]{:S(2)}, u32[]{:S(2)}) %all-to-all-start.2) | async-done | bytes 262176 | tf_op jit(solution)/shard_map/all_to_all | solution.py:465
  71.8 0.0 collective-permute-done.1.other
  71.8 0.0 copy-done
  71.8 0.0 copy-done.1
  71.8 0.0 copy-done.2
  71.9 1.4 %shard_map.315 = bf16[1024,128]{1,0:T(8,128)(2,1)} custom-call(bf16[1024,128]{1,0:T(8,128)(2,1)S(1)} %bitcast.28, bf16[1024,128]{1,0:T(8,128)(2,1)S(1)} %bitcast.23, bf16[1024,128]{1,0:T(8,128)(2,1)S(1)} %bitcast.25, bf16[128,1024]{1,0:T(8,128)(2,1)S(1)} %bitcast.27, bf16[3072,128]{1,0:T(8,128)(2,1)S(1)} %collective-permute-done.1.other), custom_call_target="tpu_custom_call" | custom-call | tf_op jit(solution)/shard_map/pallas_call | solution.py:479
  73.3 0.0 copy-start.8
  73.3 9.0 %all-to-all-start.3 = ((bf16[512,2,128]{2,1,0:T(2,128)(2,1)}), bf16[512,2,128]{2,1,0:T(2,128)(2,1)S(1)}, u32[]{:S(2)}, u32[]{:S(2)}) async-start(bf16[512,2,128]{2,1,0:T(2,128)(2,1)} %bitcast.30), calls=%async_computation.3 | async-start | bytes 524288 | tf_op jit(solution)/shard_map/all_to_all | solution.py:485
  82.3 3.3 %collective-permute-start.2 = (bf16[16,256]{1,0:T(8,128)(2,1)S(1)}, bf16[16,256]{1,0:T(8,128)(2,1)S(1)}, u32[]{:S(2)}, u32[]{:S(2)}) collective-permute-start(bf16[16,256]{1,0:T(8,128)(2,1)S(1)} %get-tuple-element.64), channel_id=1, source_target_pairs={{0,1},{1,0},{2,3},{3,2},{4,5},{5,4},{6,7},{7,6},{8,9},{9,8},{10,11... | collective-permute-start | bytes 24584 | tf_op jit(solution)/shard_map/ppermute | solution.py:477
  85.5 1.4 %collective-permute-done.2.got = bf16[16,256]{1,0:T(8,128)(2,1)S(1)} collective-permute-done((bf16[16,256]{1,0:T(8,128)(2,1)S(1)}, bf16[16,256]{1,0:T(8,128)(2,1)S(1)}, u32[]{:S(2)}, u32[]{:S(2)}) %collective-permute-start.2) | collective-permute-done | bytes 8224 | tf_op jit(solution)/shard_map/ppermute | solution.py:477
  87.0 12.2 %all-to-all-done.3 = bf16[512,2,128]{2,1,0:T(2,128)(2,1)S(1)} async-done(((bf16[512,2,128]{2,1,0:T(2,128)(2,1)}), bf16[512,2,128]{2,1,0:T(2,128)(2,1)S(1)}, u32[]{:S(2)}, u32[]{:S(2)}) %all-to-all-start.3) | async-done | bytes 262176 | tf_op jit(solution)/shard_map/all_to_all | solution.py:485
  99.1 0.0 copy-done.8
  99.1 0.8 shard_map.316
  (1 shorter events, 0.0 us)
Async XLA Ops:
  2.0 9.1 %all-to-all-start = ((bf16[4,16,256]{2,1,0:T(8,128)(2,1)}), bf16[4,16,256]{2,1,0:T(8,128)(2,1)S(1)}, u32[]{:S(2)}, u32[]{:S(2)}) async-start(bf16[4,16,256]{2,1,0:T(8,128)(2,1)} %shard_map.308), calls=%async_computation | async-start | bytes 65536 | tf_op jit(solution)/shard_map/all_to_all | solution.py:377
  6.8 4.3 %copy-start.6 = (bf16[128,1024]{1,0:T(8,128)(2,1)S(1)}, bf16[128,1024]{1,0:T(8,128)(2,1)}, u32[]{:S(2)}) copy-start(bf16[128,1024]{1,0:T(8,128)(2,1)} %proj_out.1) | copy-start | bytes 786436
  11.1 19.8 %copy-start.9 = (bf16[1024]{0:T(1024)(128)(2,1)S(1)}, bf16[1024]{0:T(1024)(128)(2,1)}, u32[]{:S(2)}) copy-start(bf16[1024]{0:T(1024)(128)(2,1)} %ffn_gain.1) | copy-start | bytes 6148
  11.1 45.5 %copy-start.5 = (bf16[1024,256]{1,0:T(8,128)(2,1)S(1)}, bf16[1024,256]{1,0:T(8,128)(2,1)}, u32[]{:S(2)}) copy-start(bf16[1024,256]{1,0:T(8,128)(2,1)} %down.1) | copy-start | bytes 1572868
  14.4 57.4 %collective-permute-start.1 = (bf16[3072,128]{1,0:T(8,128)(2,1)}, bf16[3072,128]{1,0:T(8,128)(2,1)S(1)}, u32[]{:S(2)}, u32[]{:S(2)}) collective-permute-start(bf16[3072,128]{1,0:T(8,128)(2,1)} %get-tuple-element.61), channel_id=1, source_target_pairs={{0,1},{1,0},{2,3},{3,2},{4,5},{5,4},{6,7},{7,6},{8,9},{9,8},{10,11... | collective-permute-start | bytes 2359304 | tf_op jit(solution)/shard_map/ppermute | solution.py:453
  16.6 40.0 %copy-start.4 = (bf16[1024,256]{1,0:T(8,128)(2,1)S(1)}, bf16[1024,256]{1,0:T(8,128)(2,1)}, u32[]{:S(2)}) copy-start(bf16[1024,256]{1,0:T(8,128)(2,1)} %up.1) | copy-start | bytes 1572868
  16.6 14.3 %all-to-all-start.1 = ((bf16[4,16,1024]{2,1,0:T(8,128)(2,1)}), bf16[4,16,1024]{2,1,0:T(8,128)(2,1)S(1)}, u32[]{:S(2)}, u32[]{:S(2)}) async-start(bf16[4,16,1024]{2,1,0:T(8,128)(2,1)} %get-tuple-element.50), calls=%async_computation.1 | async-start | bytes 262144 | tf_op jit(solution)/shard_map/all_to_all | solution.py:437
  20.1 36.5 %copy-start.3 = (bf16[1024,256]{1,0:T(8,128)(2,1)S(1)}, bf16[1024,256]{1,0:T(8,128)(2,1)}, u32[]{:S(2)}) copy-start(bf16[1024,256]{1,0:T(8,128)(2,1)} %gate.1) | copy-start | bytes 1572868
  21.5 10.5 %copy-start.7 = (bf16[64,1024]{1,0:T(8,128)(2,1)}, bf16[64,1024]{1,0:T(8,128)(2,1)S(1)}, u32[]{:S(2)}) copy-start(bf16[64,1024]{1,0:T(8,128)(2,1)S(1)} %get-tuple-element.62.combine) | copy-start | bytes 393220
  32.0 24.6 %copy-start.10 = (bf16[1024]{0:T(1024)(128)(2,1)S(1)}, bf16[1024]{0:T(1024)(128)(2,1)}, u32[]{:S(2)}) copy-start(bf16[1024]{0:T(1024)(128)(2,1)} %branch_gate.1) | copy-start | bytes 6148
  32.0 39.8 %all-to-all-start.2 = ((bf16[128,8,128]{2,1,0:T(8,128)(2,1)}), bf16[128,8,128]{2,1,0:T(8,128)(2,1)S(1)}, u32[]{:S(2)}, u32[]{:S(2)}) async-start(bf16[128,8,128]{2,1,0:T(8,128)(2,1)} %bitcast.31), calls=%async_computation.2 | async-start | bytes 524288 | tf_op jit(solution)/shard_map/all_to_all | solution.py:465
  56.6 15.2 %copy-start = (bf16[1,1024,128]{2,1,0:T(8,128)(2,1)S(1)}, bf16[1,1024,128]{2,1,0:T(8,128)(2,1)}, u32[]{:S(2)}) copy-start(bf16[1,1024,128]{2,1,0:T(8,128)(2,1)} %param.51) | copy-start | bytes 786436
  56.7 15.2 %copy-start.1 = (bf16[1,1024,128]{2,1,0:T(8,128)(2,1)S(1)}, bf16[1,1024,128]{2,1,0:T(8,128)(2,1)}, u32[]{:S(2)}) copy-start(bf16[1,1024,128]{2,1,0:T(8,128)(2,1)} %param.52) | copy-start | bytes 786436
  56.7 15.2 %copy-start.2 = (bf16[1,128,1024]{2,1,0:T(8,128)(2,1)S(1)}, bf16[1,128,1024]{2,1,0:T(8,128)(2,1)}, u32[]{:S(2)}) copy-start(bf16[1,128,1024]{2,1,0:T(8,128)(2,1)} %param.53) | copy-start | bytes 786436
  57.1 6.3 %collective-permute-start = (bf16[16,512]{1,0:T(8,128)(2,1)S(1)}, bf16[16,512]{1,0:T(8,128)(2,1)S(1)}, u32[]{:S(2)}, u32[]{:S(2)}) collective-permute-start(bf16[16,512]{1,0:T(8,128)(2,1)S(1)} %get-tuple-element.58), channel_id=1, source_target_pairs={{0,2},{1,3},{2,0},{3,1},{4,6},{5,7},{6,4},{7,5},{8,10},{9,11},{10,... | collective-permute-start | bytes 49160 | tf_op jit(solution)/shard_map/ppermute | solution.py:472
  73.3 25.9 %copy-start.8 = (bf16[64,1024]{1,0:T(8,128)(2,1)S(1)}, bf16[64,1024]{1,0:T(8,128)(2,1)}, u32[]{:S(2)}) copy-start(bf16[64,1024]{1,0:T(8,128)(2,1)} %copy-done.7) | copy-start | bytes 393220
  73.3 25.9 %all-to-all-start.3 = ((bf16[512,2,128]{2,1,0:T(2,128)(2,1)}), bf16[512,2,128]{2,1,0:T(2,128)(2,1)S(1)}, u32[]{:S(2)}, u32[]{:S(2)}) async-start(bf16[512,2,128]{2,1,0:T(2,128)(2,1)} %bitcast.30), calls=%async_computation.3 | async-start | bytes 524288 | tf_op jit(solution)/shard_map/all_to_all | solution.py:485
  82.3 4.7 %collective-permute-start.2 = (bf16[16,256]{1,0:T(8,128)(2,1)S(1)}, bf16[16,256]{1,0:T(8,128)(2,1)S(1)}, u32[]{:S(2)}, u32[]{:S(2)}) collective-permute-start(bf16[16,256]{1,0:T(8,128)(2,1)S(1)} %get-tuple-element.64), channel_id=1, source_target_pairs={{0,1},{1,0},{2,3},{3,2},{4,5},{5,4},{6,7},{7,6},{8,9},{9,8},{10,11... | collective-permute-start | bytes 24584 | tf_op jit(solution)/shard_map/ppermute | solution.py:477
where the time goes:
time: 100 us; the launch traced here: 99.9 us
  starting transfers between devices  50.5 us (50%)
  waiting for transfers between devices  36.7 us (37%)
  Pallas kernels  11.9 us (12%)
    all_to_all x1, starting transfers between devices, local(): lax.all_to_all(outgoing.reshape(eps, pieces, 128), 'ep', 0, 0, tiled=True)  24.6 us
    all_to_all x1, waiting for transfers between devices, local(): lax.all_to_all(results.reshape(tps * eps, 2, 128), ('tp', 'ep'), 0, 0, ti...  12.2 us
    all_to_all x1, waiting for transfers between devices, local(): mixed_in = lax.all_to_all(partial, 'tp', 0, 0, tiled=True)  9.46 us
    all_to_all x1, starting transfers between devices, local(): lax.all_to_all(results.reshape(tps * eps, 2, 128), ('tp', 'ep'), 0, 0, ti...  8.98 us
    all_to_all x1, waiting for transfers between devices, local(): lax.all_to_all(outgoing.reshape(eps, pieces, 128), 'ep', 0, 0, tiled=True)  8.41 us
    all_to_all x1, starting transfers between devices, local(): arrived = lax.all_to_all(spread, 'tp', 0, 0, tiled=True)  4.84 us
    all_to_all x1, starting transfers between devices, local(): mixed_in = lax.all_to_all(partial, 'tp', 0, 0, tiled=True)  3.47 us
    pallas_call x1, Pallas kernels, local(): call(mixer_body, (pltpu.HBM((tps, rows, width), BF16), sds((rows, inner,...  3.29 us
  transfers between devices with their start and end apart: 7, of which 6 were waited for; matrix products, arithmetic and copies ran while one was open for 0% of the time, Pallas kernels for 5%

commit v1 on v0

--- a/solution.py
+++ b/solution.py
@@ -75,34 +75,36 @@
     return test(down, across).astype(F32).astype(BF16)
 
 
-def route_body(rank, ids_there, weights_there, select, combine, ids, weights, sems):
-    copies = [
-        pltpu.make_async_copy(ids_there, ids, sems.at[0]),
-        pltpu.make_async_copy(weights_there, weights, sems.at[1]),
-    ]
-    for copy in copies:
-        copy.start()
-    for copy in copies:
-        copy.wait()
+def places(ids, experts):
     tops, rows = ids.shape
-    experts = combine.shape[1] // 8
-    pieces = select.shape[0] // experts
     expert = lax.broadcasted_iota(jnp.int32, (experts, rows), 0)
+    same = [expert == ids[k : k + 1, :] for k in range(tops)]
     hits = jnp.zeros((experts, rows), F32)
-    amount = jnp.zeros((experts, rows), F32)
-    for k in range(tops):
-        same = expert == ids[k : k + 1, :]
-        hits = jnp.where(same, 1.0, hits)
-        amount = jnp.where(same, weights[k : k + 1, :], amount)
+    for match in same:
+        hits = jnp.where(match, 1.0, hits)
     earlier = zeros_and_ones((rows, rows), lambda d, a: d < a)
-    place = nn(hits.astype(BF16), earlier)
+    return same, hits, nn(hits.astype(BF16), earlier)
+
+
+def selection(rank, ids, experts, pieces):
+    rows = ids.shape[1]
+    _, hits, place = places(ids, experts)
     mine = jnp.bitwise_and(rank[0], 1).astype(F32)
     chosen = jnp.where(place == mine, hits, 0.0).astype(BF16)
     down = zeros_and_ones((experts * pieces, experts), lambda d, a: d // pieces == a)
     across = zeros_and_ones((rows, rows * pieces), lambda d, a: a // pieces == d)
-    wide = nn(nn(down, chosen).astype(BF16), across)
+    wide = nn(down, nn(chosen, across).astype(BF16))
     matched = zeros_and_ones(wide.shape, lambda d, a: d % pieces == a % pieces)
-    select[...] = wide.astype(BF16) * matched
+    return wide.astype(BF16) * matched
+
+
+def weigh_body(ids, weights, combine):
+    tops, rows = ids.shape
+    experts = combine.shape[1] // 8
+    same, _, place = places(ids, experts)
+    amount = jnp.zeros((experts, rows), F32)
+    for k in range(tops):
+        amount = jnp.where(same[k], weights[k : k + 1, :], amount)
     twice = zeros_and_ones((experts, experts * 2), lambda d, a: a // 2 == d)
     halves = lax.broadcasted_iota(jnp.int32, (rows, experts * 2), 1) % 2
     for s in range(2):
@@ -113,11 +115,11 @@
             both = nn(piece, twice)
             for h in range(2):
                 rows_at = (2 * p + h) * rows
-                kept = jnp.where(halves == h, both, 0.0).astype(BF16)
+                kept_half = jnp.where(halves == h, both, 0.0).astype(BF16)
                 for t in (s, s + 2):
                     combine[
                         rows_at : rows_at + rows, t * 2 * experts : (t + 1) * 2 * experts
-                    ] = kept
+                    ] = kept_half
 
 
 STAGED = 9
@@ -202,6 +204,8 @@
     new_input_window,
     new_write_window,
     new_read_window,
+    fresh_state,
+    sems,
 ):
     rows = arrived.shape[1]
     x = jnp.concatenate([arrived[j] for j in range(arrived.shape[0])], axis=1).astype(F32)
@@ -238,9 +242,11 @@
         fresh = (
             decay_t[:, b : b + 1] * state[b] + scaled_t[:, b : b + 1] * write_conv[b : b + 1, :]
         )
-        new_state[b] = fresh
+        fresh_state[b] = fresh
         seen = jnp.sum(fresh * read_conv[b : b + 1, :], axis=1, keepdims=True)
         readout_t = jnp.where(lane == b, seen, readout_t)
+    state_copy = pltpu.make_async_copy(fresh_state, new_state, sems.at[0])
+    state_copy.start()
     readout = readout_t.T + lanes[2:3, :] * input_conv
     gated = readout * silu(gate_rows.astype(F32))
     gated = gated * lax.rsqrt(jnp.mean(gated * gated, axis=-1, keepdims=True) + EPS)
@@ -248,12 +254,15 @@
     mixed = nn(mixer_rows, proj_out[...]).astype(BF16)
     for j in range(partial.shape[0]):
         partial[j] = mixed
+    state_copy.wait()
 
 
 def hidden_body(
-    rank, arrived, mixed_in, ffn_gain, select, outgoing, normed_out, hidden_part, folded
+    rank, arrived, mixed_in, ffn_gain, ids, outgoing, normed_out, hidden_part, folded
 ):
     count, rows, quarter = arrived.shape
+    pieces = folded.shape[0] // rows
+    select = selection(rank, ids, outgoing.shape[0] // pieces, pieces)
     x = jnp.concatenate([arrived[j] for j in range(count)], axis=1).astype(F32)
     mixed = mixed_in[0].astype(F32)
     for j in range(1, count):
@@ -263,10 +272,9 @@
     scale = lax.rsqrt(jnp.mean(wide * wide, axis=-1, keepdims=True) + EPS)
     normed_wide = wide * scale * ffn_gain[...].astype(F32)[None, :]
     normed_out[...] = normed_wide.astype(BF16)
-    pieces = folded.shape[0] // rows
     for j in range(pieces):
         folded[pl.ds(j, rows, stride=pieces), :] = normed_wide[:, j * 128 : (j + 1) * 128]
-    outgoing[...] = nn(select[...], folded[...].astype(BF16)).astype(BF16)
+    outgoing[...] = nn(select, folded[...].astype(BF16)).astype(BF16)
     part = wide[:, 0:quarter]
     for j in range(1, count):
         part = jnp.where(rank[0] == j, wide[:, j * quarter : (j + 1) * quarter], part)
@@ -433,23 +441,11 @@
             sds((3, rows, latent), BF16),
         ),
         [SMEM] + [VMEM] * 14,
+        [pltpu.VMEM((rows, inner, STATE), F32), pltpu.SemaphoreType.DMA((1,))],
+        (VMEM, HBM, VMEM, VMEM, VMEM),
     )(rank, lanes, arrived, *staged, proj_out)
     mixed_in = lax.all_to_all(partial, "tp", 0, 0, tiled=True)
-    ids, weights = expert_ids.T, expert_weights.T
-    packed, ids, weights, _ = lax.optimization_barrier((packed, ids, weights, partial))
-    select, combine = call(
-        route_body,
-        (
-            sds((eps * pieces, rows * pieces), BF16),
-            sds((4 * rows, 2 * tps * eps), BF16),
-        ),
-        [SMEM, HBM, HBM],
-        [
-            pltpu.VMEM(ids.shape, ids.dtype),
-            pltpu.VMEM(weights.shape, F32),
-            pltpu.SemaphoreType.DMA((2,)),
-        ],
-    )(rank, kept(ids), kept(weights))
+    packed, _ = lax.optimization_barrier((packed, partial))
     other = lax.ppermute(packed, "tp", [(t, t ^ 1) for t in range(tps)])
 
     outgoing, normed_ffn, hidden_part = call(
@@ -461,9 +457,13 @@
         ),
         [SMEM] + [VMEM] * 4,
         [pltpu.VMEM((rows * pieces, 128), F32)],
-    )(rank, arrived, mixed_in, ffn_gain, select)
+    )(rank, arrived, mixed_in, ffn_gain, expert_ids.T)
     items = lax.all_to_all(outgoing.reshape(eps, pieces, 128), "ep", 0, 0, tiled=True)
 
+    ids, weights, normed_ffn = lax.optimization_barrier(
+        (expert_ids.T, expert_weights.T, normed_ffn)
+    )
+    combine = call(weigh_body, sds((4 * rows, 2 * tps * eps), BF16), [VMEM] * 2)(ids, weights)
     give, keep, branch = call(
         dense_body,
         (sds((rows, width // 2), BF16), sds((rows, width // 2), BF16), sds((rows, 128), F32)),

time: 100 us -> 102 us (1.020)
  blocking collectives: 0 us -> 14.3 us
  waiting for transfers between devices: 36.7 us -> 26.3 us
  starting transfers between devices: 50.5 us -> 47.6 us
    all_to_all x0 -> x1, blocking collectives: none -> 14.3 us  [local(): mixed_in = lax.all_to_all(partial, 'tp', 0, 0, tiled=True)]
    all_to_all x1 -> x0, waiting for transfers between devices: 9.46 us -> none  [local(): mixed_in = lax.all_to_all(partial, 'tp', 0, 0, tiled=True)]
    all_to_all x1 -> x0, starting transfers between devices: 3.47 us -> none  [local(): mixed_in = lax.all_to_all(partial, 'tp', 0, 0, tiled=True)]
  transfers between devices with their start and end apart: 7 -> 6, of which waited for: 6 -> 5; matrix products, arithmetic and copies ran while one was open for 0% -> 0% of each run, Pallas kernels for 5% -> 4%
where the time goes in v1:
time: 102 us; the launch traced here: 101 us
  starting transfers between devices  47.6 us (47%)
  waiting for transfers between devices  26.3 us (26%)
  blocking collectives  14.3 us (14%)
  Pallas kernels  11.7 us (11%)
    all_to_all x1, starting transfers between devices, local(): lax.all_to_all(outgoing.reshape(eps, pieces, 128), 'ep', 0, 0, tiled=True)  24.5 us
    all_to_all x1, blocking collectives, local(): mixed_in = lax.all_to_all(partial, 'tp', 0, 0, tiled=True)  14.3 us
    all_to_all x1, waiting for transfers between devices, local(): lax.all_to_all(results.reshape(tps * eps, 2, 128), ('tp', 'ep'), 0, 0, ti...  12.2 us
    all_to_all x1, starting transfers between devices, local(): lax.all_to_all(results.reshape(tps * eps, 2, 128), ('tp', 'ep'), 0, 0, ti...  9.59 us
    all_to_all x1, waiting for transfers between devices, local(): lax.all_to_all(outgoing.reshape(eps, pieces, 128), 'ep', 0, 0, tiled=True)  7.8 us
    all_to_all x1, starting transfers between devices, local(): arrived = lax.all_to_all(spread, 'tp', 0, 0, tiled=True)  4.84 us
    pallas_call x1, Pallas kernels, local(): call(mixer_body, (pltpu.HBM((tps, rows, width), BF16), sds((rows, inner,...  3.74 us
    ppermute x1, starting transfers between devices, local(): got = lax.ppermute(give, 'tp', [(t, t ^ 1) for t in range(tps)])  3.26 us
  transfers between devices with their start and end apart: 6, of which 5 were waited for; matrix products, arithmetic and copies ran while one was open for 0% of the time, Pallas kernels for 4%

profile of v1, /device:TPU:1, one launch (start us, length us, event | category | flops | bytes accessed | tf_op | source)
XLA Modules:
  0.0 101.4 jit_solution(17011040185447901597)
XLA Ops:
  0.6 1.3 %shard_map.308 = bf16[4,16,256]{2,1,0:T(8,128)(2,1)} custom-call(bf16[16,256]{1,0:T(8,128)(2,1)} %tokens.1), custom_call_target="tpu_custom_call" | custom-call | tf_op jit(solution)/shard_map/pallas_call | solution.py:378
  2.0 4.8 %all-to-all-start = ((bf16[4,16,256]{2,1,0:T(8,128)(2,1)}), bf16[4,16,256]{2,1,0:T(8,128)(2,1)S(1)}, u32[]{:S(2)}, u32[]{:S(2)}) async-start(bf16[4,16,256]{2,1,0:T(8,128)(2,1)} %shard_map.308), calls=%async_computation | async-start | bytes 65536 | tf_op jit(solution)/shard_map/all_to_all | solution.py:385
  6.8 0.0 copy-start.6
  6.8 2.2 %shard_map.309 = (f32[8,128]{1,0:T(8,128)S(1)}, bf16[3072,128]{1,0:T(8,128)(2,1)}, bf16[1024,256]{1,0:T(8,128)(2,1)S(1)}, bf16[136,1024]{1,0:T(8,128)(2,1)S(1)},...) custom-call(s32[1]{0:T(128)} %bitcast.refs_0_.rank, ...), custom_call_target="tpu_custom_call" | custom-call | tf_op jit(solution)/shard_map/pallas_call | solution.py:399
  9.1 2.1 %all-to-all-done.arrived = bf16[4,16,256]{2,1,0:T(8,128)(2,1)S(1)} async-done(((bf16[4,16,256]{2,1,0:T(8,128)(2,1)}), bf16[4,16,256]{2,1,0:T(8,128)(2,1)S(1)}, u32[]{:S(2)}, u32[]{:S(2)}) %all-to-all-start) | async-done | bytes 32800 | tf_op jit(solution)/shard_map/all_to_all | solution.py:385
  11.1 0.0 copy-done.6
  11.1 0.0 copy-start.7
  11.1 0.0 copy-start.9
  11.1 0.0 copy-start.4
  11.1 0.0 copy-start.5
  11.2 3.7 %shard_map.310 = (bf16[4,16,1024]{2,1,0:T(8,128)(2,1)}, f32[16,128,64]{2,1,0:T(8,128)}, bf16[3,16,128]{2,1,0:T(8,128)(2,1)}, bf16[3,16,64]{2,1,0:T(8,128)(2,1)}, bf16[3,16,64]{2,1,0:T(8,128)(2,1)}) custom-call(s32[1]{0:T(128)} %bitcast.refs_0_.rank, f32[8,128]{1,0:T(8,128)S(1)} %get-tuple-element.37.lanes, bf16[4,16,256]{2,1,0:T(8,128)(2,1)S(1)} %all-to-all-done.arrived, ...), custom_call_target="tpu_custom_call" | custom-call | tf_op jit(solution)/shard_map/pallas_call | solution.py:434
  14.9 0.0 copy-start.3
  14.9 2.3 %collective-permute-start.1 = (bf16[3072,128]{1,0:T(8,128)(2,1)}, bf16[3072,128]{1,0:T(8,128)(2,1)S(1)}, u32[]{:S(2)}, u32[]{:S(2)}) collective-permute-start(bf16[3072,128]{1,0:T(8,128)(2,1)} %get-tuple-element.58), channel_id=1, source_target_pairs={{0,1},{1,0},{2,3},{3,2},{4,5},{5,4},{6,7},{7,6},{8,9},{9,8},{10,11... | collective-permute-start | bytes 2359304 | tf_op jit(solution)/shard_map/ppermute | solution.py:449
  17.3 14.3 %all_to_all.20.mixed_in = bf16[4,16,1024]{2,1,0:T(8,128)(2,1)S(1)} all-to-all(bf16[4,16,1024]{2,1,0:T(8,128)(2,1)} %get-tuple-element.49), channel_id=1, replica_groups=mesh['ep'=128,'tp'=4] {'tp'}, dimensions={0} | all-to-all | bytes 262144 | tf_op jit(solution)/shard_map/all_to_all | solution.py:447
  31.6 0.0 copy-done.7
  31.6 0.0 copy-done.9
  31.6 1.4 %shard_map.311 = (bf16[1024,128]{1,0:T(8,128)(2,1)}, bf16[16,1024]{1,0:T(8,128)(2,1)S(1)}, bf16[16,256]{1,0:T(8,128)(2,1)S(1)}) custom-call(s32[1]{0:T(128)} %bitcast.refs_0_.rank, bf16[4,16,256]{2,1,0:T(8,128)(2,1)S(1)} %all-to-all-done.arrived, bf16[4,16,1024]{2,1,0:T(8,128)(2,1)S(1)} %all_to_all.20.mixed_in, bf16[1024]{0:T(1024)(128)(2,1)S(1)} %copy-done.9, ...), custom_call_target="tpu_custom_call" | custom-call | tf_op jit(solution)/shard_map/pallas_call | solution.py:451
  32.9 24.5 %all-to-all-start.2 = ((bf16[128,8,128]{2,1,0:T(8,128)(2,1)}), bf16[128,8,128]{2,1,0:T(8,128)(2,1)S(1)}, u32[]{:S(2)}, u32[]{:S(2)}) async-start(bf16[128,8,128]{2,1,0:T(8,128)(2,1)} %bitcast.34), calls=%async_computation.2 | async-start | bytes 524288 | tf_op jit(solution)/shard_map/all_to_all | solution.py:461
  57.4 0.0 copy-start.10
  57.4 0.0 copy-done.4
  57.4 0.0 copy-done.5
  57.4 0.0 copy-done.3
  57.5 0.6 copy-done.10
  58.1 0.0 copy-start
  58.1 0.0 copy-start.1
  58.1 0.0 copy-start.2
  58.1 0.4 shard_map.312
  58.5 3.1 %collective-permute-start = (bf16[16,512]{1,0:T(8,128)(2,1)S(1)}, bf16[16,512]{1,0:T(8,128)(2,1)S(1)}, u32[]{:S(2)}, u32[]{:S(2)}) collective-permute-start(bf16[16,512]{1,0:T(8,128)(2,1)S(1)} %get-tuple-element.54), channel_id=1, source_target_pairs={{0,2},{1,3},{2,0},{3,1},{4,6},{5,7},{6,4},{7,5},{8,10},{9,11},{10,... | collective-permute-start | bytes 49160 | tf_op jit(solution)/shard_map/ppermute | solution.py:472
  61.6 3.2 %collective-permute-done.got = bf16[16,512]{1,0:T(8,128)(2,1)S(1)} collective-permute-done((bf16[16,512]{1,0:T(8,128)(2,1)S(1)}, bf16[16,512]{1,0:T(8,128)(2,1)S(1)}, u32[]{:S(2)}, u32[]{:S(2)}) %collective-permute-start) | collective-permute-done | bytes 16416 | tf_op jit(solution)/shard_map/ppermute | solution.py:472
  64.8 7.8 %all-to-all-done.2 = bf16[128,8,128]{2,1,0:T(8,128)(2,1)S(1)} async-done(((bf16[128,8,128]{2,1,0:T(8,128)(2,1)}), bf16[128,8,128]{2,1,0:T(8,128)(2,1)S(1)}, u32[]{:S(2)}, u32[]{:S(2)}) %all-to-all-start.2) | async-done | bytes 262176 | tf_op jit(solution)/shard_map/all_to_all | solution.py:461
  72.6 0.0 collective-permute-done.1.other
  72.6 0.0 copy-done
  72.6 0.0 copy-done.1
  72.7 0.0 copy-done.2
  72.7 1.4 %shard_map.314 = bf16[1024,128]{1,0:T(8,128)(2,1)} custom-call(bf16[1024,128]{1,0:T(8,128)(2,1)S(1)} %bitcast.28, bf16[1024,128]{1,0:T(8,128)(2,1)S(1)} %bitcast.23, bf16[1024,128]{1,0:T(8,128)(2,1)S(1)} %bitcast.25, bf16[128,1024]{1,0:T(8,128)(2,1)S(1)} %bitcast.27, bf16[3072,128]{1,0:T(8,128)(2,1)S(1)} %collective-permute-done.1.other), custom_call_target="tpu_custom_call" | custom-call | tf_op jit(solution)/shard_map/pallas_call | solution.py:479
  74.1 0.0 copy-start.8
  74.1 9.6 %all-to-all-start.3 = ((bf16[512,2,128]{2,1,0:T(2,128)(2,1)}), bf16[512,2,128]{2,1,0:T(2,128)(2,1)S(1)}, u32[]{:S(2)}, u32[]{:S(2)}) async-start(bf16[512,2,128]{2,1,0:T(2,128)(2,1)} %bitcast.33), calls=%async_computation.3 | async-start | bytes 524288 | tf_op jit(solution)/shard_map/all_to_all | solution.py:485
  83.7 3.3 %collective-permute-start.2 = (bf16[16,256]{1,0:T(8,128)(2,1)S(1)}, bf16[16,256]{1,0:T(8,128)(2,1)S(1)}, u32[]{:S(2)}, u32[]{:S(2)}) collective-permute-start(bf16[16,256]{1,0:T(8,128)(2,1)S(1)} %get-tuple-element.62), channel_id=1, source_target_pairs={{0,1},{1,0},{2,3},{3,2},{4,5},{5,4},{6,7},{7,6},{8,9},{9,8},{10,11... | collective-permute-start | bytes 24584 | tf_op jit(solution)/shard_map/ppermute | solution.py:477
  87.0 0.0 copy-done.8
  87.0 0.4 shard_map.315.combine
  87.3 1.1 %collective-permute-done.2.got = bf16[16,256]{1,0:T(8,128)(2,1)S(1)} collective-permute-done((bf16[16,256]{1,0:T(8,128)(2,1)S(1)}, bf16[16,256]{1,0:T(8,128)(2,1)S(1)}, u32[]{:S(2)}, u32[]{:S(2)}) %collective-permute-start.2) | collective-permute-done | bytes 8224 | tf_op jit(solution)/shard_map/ppermute | solution.py:477
  88.4 12.2 %all-to-all-done.3 = bf16[512,2,128]{2,1,0:T(2,128)(2,1)S(1)} async-done(((bf16[512,2,128]{2,1,0:T(2,128)(2,1)}), bf16[512,2,128]{2,1,0:T(2,128)(2,1)S(1)}, u32[]{:S(2)}, u32[]{:S(2)}) %all-to-all-start.3) | async-done | bytes 262176 | tf_op jit(solution)/shard_map/all_to_all | solution.py:485
  100.6 0.8 shard_map.316
  (1 shorter events, 0.0 us)
Async XLA Ops:
  2.0 9.1 %all-to-all-start = ((bf16[4,16,256]{2,1,0:T(8,128)(2,1)}), bf16[4,16,256]{2,1,0:T(8,128)(2,1)S(1)}, u32[]{:S(2)}, u32[]{:S(2)}) async-start(bf16[4,16,256]{2,1,0:T(8,128)(2,1)} %shard_map.308), calls=%async_computation | async-start | bytes 65536 | tf_op jit(solution)/shard_map/all_to_all | solution.py:385
  6.8 4.3 %copy-start.6 = (bf16[128,1024]{1,0:T(8,128)(2,1)S(1)}, bf16[128,1024]{1,0:T(8,128)(2,1)}, u32[]{:S(2)}) copy-start(bf16[128,1024]{1,0:T(8,128)(2,1)} %proj_out.1) | copy-start | bytes 786436
  11.1 20.5 %copy-start.7 = (s32[16,6]{0,1:T(8,128)S(1)}, s32[16,6]{0,1:T(8,128)}, u32[]{:S(2)}) copy-start(s32[16,6]{0,1:T(8,128)} %param.49) | copy-start | bytes 1156
  11.1 20.5 %copy-start.9 = (bf16[1024]{0:T(1024)(128)(2,1)S(1)}, bf16[1024]{0:T(1024)(128)(2,1)}, u32[]{:S(2)}) copy-start(bf16[1024]{0:T(1024)(128)(2,1)} %ffn_gain.1) | copy-start | bytes 6148
  11.1 46.3 %copy-start.4 = (bf16[1024,256]{1,0:T(8,128)(2,1)S(1)}, bf16[1024,256]{1,0:T(8,128)(2,1)}, u32[]{:S(2)}) copy-start(bf16[1024,256]{1,0:T(8,128)(2,1)} %up.1) | copy-start | bytes 1572868
  11.1 46.3 %copy-start.5 = (bf16[1024,256]{1,0:T(8,128)(2,1)S(1)}, bf16[1024,256]{1,0:T(8,128)(2,1)}, u32[]{:S(2)}) copy-start(bf16[1024,256]{1,0:T(8,128)(2,1)} %down.1) | copy-start | bytes 1572868
  14.9 42.5 %copy-start.3 = (bf16[1024,256]{1,0:T(8,128)(2,1)S(1)}, bf16[1024,256]{1,0:T(8,128)(2,1)}, u32[]{:S(2)}) copy-start(bf16[1024,256]{1,0:T(8,128)(2,1)} %gate.1) | copy-start | bytes 1572868
  14.9 57.7 %collective-permute-start.1 = (bf16[3072,128]{1,0:T(8,128)(2,1)}, bf16[3072,128]{1,0:T(8,128)(2,1)S(1)}, u32[]{:S(2)}, u32[]{:S(2)}) collective-permute-start(bf16[3072,128]{1,0:T(8,128)(2,1)} %get-tuple-element.58), channel_id=1, source_target_pairs={{0,1},{1,0},{2,3},{3,2},{4,5},{5,4},{6,7},{7,6},{8,9},{9,8},{10,11... | collective-permute-start | bytes 2359304 | tf_op jit(solution)/shard_map/ppermute | solution.py:449
  32.9 39.7 %all-to-all-start.2 = ((bf16[128,8,128]{2,1,0:T(8,128)(2,1)}), bf16[128,8,128]{2,1,0:T(8,128)(2,1)S(1)}, u32[]{:S(2)}, u32[]{:S(2)}) async-start(bf16[128,8,128]{2,1,0:T(8,128)(2,1)} %bitcast.34), calls=%async_computation.2 | async-start | bytes 524288 | tf_op jit(solution)/shard_map/all_to_all | solution.py:461
  57.4 0.7 copy-start.10
  58.1 14.6 %copy-start = (bf16[1,1024,128]{2,1,0:T(8,128)(2,1)S(1)}, bf16[1,1024,128]{2,1,0:T(8,128)(2,1)}, u32[]{:S(2)}) copy-start(bf16[1,1024,128]{2,1,0:T(8,128)(2,1)} %param.51) | copy-start | bytes 786436
  58.1 14.6 %copy-start.1 = (bf16[1,1024,128]{2,1,0:T(8,128)(2,1)S(1)}, bf16[1,1024,128]{2,1,0:T(8,128)(2,1)}, u32[]{:S(2)}) copy-start(bf16[1,1024,128]{2,1,0:T(8,128)(2,1)} %param.52) | copy-start | bytes 786436
  58.1 14.6 %copy-start.2 = (bf16[1,128,1024]{2,1,0:T(8,128)(2,1)S(1)}, bf16[1,128,1024]{2,1,0:T(8,128)(2,1)}, u32[]{:S(2)}) copy-start(bf16[1,128,1024]{2,1,0:T(8,128)(2,1)} %param.53) | copy-start | bytes 786436
  58.5 6.3 %collective-permute-start = (bf16[16,512]{1,0:T(8,128)(2,1)S(1)}, bf16[16,512]{1,0:T(8,128)(2,1)S(1)}, u32[]{:S(2)}, u32[]{:S(2)}) collective-permute-start(bf16[16,512]{1,0:T(8,128)(2,1)S(1)} %get-tuple-element.54), channel_id=1, source_target_pairs={{0,2},{1,3},{2,0},{3,1},{4,6},{5,7},{6,4},{7,5},{8,10},{9,11},{10,... | collective-permute-start | bytes 49160 | tf_op jit(solution)/shard_map/ppermute | solution.py:472
  74.1 12.9 %copy-start.8 = (f32[16,6]{0,1:T(8,128)S(1)}, f32[16,6]{0,1:T(8,128)}, u32[]{:S(2)}) copy-start(f32[16,6]{0,1:T(8,128)} %param.50) | copy-start | bytes 1156
  74.1 26.5 %all-to-all-start.3 = ((bf16[512,2,128]{2,1,0:T(2,128)(2,1)}), bf16[512,2,128]{2,1,0:T(2,128)(2,1)S(1)}, u32[]{:S(2)}, u32[]{:S(2)}) async-start(bf16[512,2,128]{2,1,0:T(2,128)(2,1)} %bitcast.33), calls=%async_computation.3 | async-start | bytes 524288 | tf_op jit(solution)/shard_map/all_to_all | solution.py:485
  83.7 4.7 %collective-permute-start.2 = (bf16[16,256]{1,0:T(8,128)(2,1)S(1)}, bf16[16,256]{1,0:T(8,128)(2,1)S(1)}, u32[]{:S(2)}, u32[]{:S(2)}) collective-permute-start(bf16[16,256]{1,0:T(8,128)(2,1)S(1)} %get-tuple-element.62), channel_id=1, source_target_pairs={{0,1},{1,0},{2,3},{3,2},{4,5},{5,4},{6,7},{7,6},{8,9},{9,8},{10,11... | collective-permute-start | bytes 24584 | tf_op jit(solution)/shard_map/ppermute | solution.py:477

commit v2 on v1

--- a/solution.py
+++ b/solution.py
@@ -86,8 +86,10 @@
     return same, hits, nn(hits.astype(BF16), earlier)
 
 
-def selection(rank, ids, experts, pieces):
+def select_body(rank, ids, select):
     rows = ids.shape[1]
+    pieces = select.shape[1] // rows
+    experts = select.shape[0] // pieces
     _, hits, place = places(ids, experts)
     mine = jnp.bitwise_and(rank[0], 1).astype(F32)
     chosen = jnp.where(place == mine, hits, 0.0).astype(BF16)
@@ -95,10 +97,10 @@
     across = zeros_and_ones((rows, rows * pieces), lambda d, a: a // pieces == d)
     wide = nn(down, nn(chosen, across).astype(BF16))
     matched = zeros_and_ones(wide.shape, lambda d, a: d % pieces == a % pieces)
-    return wide.astype(BF16) * matched
-
-
-def weigh_body(ids, weights, combine):
+    select[...] = wide.astype(BF16) * matched
+
+
+def weigh_body(ids, weights, normed, branch_gate, combine, branch):
     tops, rows = ids.shape
     experts = combine.shape[1] // 8
     same, _, place = places(ids, experts)
@@ -120,6 +122,9 @@
                     combine[
                         rows_at : rows_at + rows, t * 2 * experts : (t + 1) * 2 * experts
                     ] = kept_half
+    scaled = normed[...].astype(F32) * branch_gate[...].astype(F32)[None, :]
+    level = jnp.sum(scaled, axis=-1, keepdims=True)
+    branch[...] = jnp.broadcast_to(jax.nn.sigmoid(level), branch.shape)
 
 
 STAGED = 9
@@ -204,8 +209,6 @@
     new_input_window,
     new_write_window,
     new_read_window,
-    fresh_state,
-    sems,
 ):
     rows = arrived.shape[1]
     x = jnp.concatenate([arrived[j] for j in range(arrived.shape[0])], axis=1).astype(F32)
@@ -242,11 +245,9 @@
         fresh = (
             decay_t[:, b : b + 1] * state[b] + scaled_t[:, b : b + 1] * write_conv[b : b + 1, :]
         )
-        fresh_state[b] = fresh
+        new_state[b] = fresh
         seen = jnp.sum(fresh * read_conv[b : b + 1, :], axis=1, keepdims=True)
         readout_t = jnp.where(lane == b, seen, readout_t)
-    state_copy = pltpu.make_async_copy(fresh_state, new_state, sems.at[0])
-    state_copy.start()
     readout = readout_t.T + lanes[2:3, :] * input_conv
     gated = readout * silu(gate_rows.astype(F32))
     gated = gated * lax.rsqrt(jnp.mean(gated * gated, axis=-1, keepdims=True) + EPS)
@@ -254,15 +255,13 @@
     mixed = nn(mixer_rows, proj_out[...]).astype(BF16)
     for j in range(partial.shape[0]):
         partial[j] = mixed
-    state_copy.wait()
 
 
 def hidden_body(
-    rank, arrived, mixed_in, ffn_gain, ids, outgoing, normed_out, hidden_part, folded
+    rank, arrived, mixed_in, ffn_gain, select, outgoing, normed_out, hidden_part, folded
 ):
     count, rows, quarter = arrived.shape
     pieces = folded.shape[0] // rows
-    select = selection(rank, ids, outgoing.shape[0] // pieces, pieces)
     x = jnp.concatenate([arrived[j] for j in range(count)], axis=1).astype(F32)
     mixed = mixed_in[0].astype(F32)
     for j in range(1, count):
@@ -274,14 +273,14 @@
     normed_out[...] = normed_wide.astype(BF16)
     for j in range(pieces):
         folded[pl.ds(j, rows, stride=pieces), :] = normed_wide[:, j * 128 : (j + 1) * 128]
-    outgoing[...] = nn(select, folded[...].astype(BF16)).astype(BF16)
+    outgoing[...] = nn(select[...], folded[...].astype(BF16)).astype(BF16)
     part = wide[:, 0:quarter]
     for j in range(1, count):
         part = jnp.where(rank[0] == j, wide[:, j * quarter : (j + 1) * quarter], part)
     hidden_part[...] = part.astype(BF16)
 
 
-def dense_body(rank, normed_in, gate, up, down, branch_gate, give, keep, branch):
+def dense_body(rank, normed_in, gate, up, down, give, keep):
     normed = normed_in[...]
     hidden = (silu(nn(normed, gate[...])) * nn(normed, up[...])).astype(BF16)
     total = nt(hidden, down[...]).astype(BF16)
@@ -289,10 +288,6 @@
     upper = rank[0] > 1
     give[...] = jnp.where(upper, total[:, 0:half], total[:, half:])
     keep[...] = jnp.where(upper, total[:, half:], total[:, 0:half])
-    level = jnp.sum(
-        normed.astype(F32) * branch_gate[...].astype(F32)[None, :], axis=-1, keepdims=True
-    )
-    branch[...] = jnp.broadcast_to(jax.nn.sigmoid(level), branch.shape)
 
 
 def halve_body(rank, keep, got, give, left):
@@ -441,11 +436,10 @@
             sds((3, rows, latent), BF16),
         ),
         [SMEM] + [VMEM] * 14,
-        [pltpu.VMEM((rows, inner, STATE), F32), pltpu.SemaphoreType.DMA((1,))],
-        (VMEM, HBM, VMEM, VMEM, VMEM),
     )(rank, lanes, arrived, *staged, proj_out)
     mixed_in = lax.all_to_all(partial, "tp", 0, 0, tiled=True)
-    packed, _ = lax.optimization_barrier((packed, partial))
+    packed, ids, _ = lax.optimization_barrier((packed, expert_ids.T, partial))
+    select = call(select_body, sds((eps * pieces, rows * pieces), BF16), [SMEM, VMEM])(rank, ids)
     other = lax.ppermute(packed, "tp", [(t, t ^ 1) for t in range(tps)])
 
     outgoing, normed_ffn, hidden_part = call(
@@ -457,18 +451,20 @@
         ),
         [SMEM] + [VMEM] * 4,
         [pltpu.VMEM((rows * pieces, 128), F32)],
-    )(rank, arrived, mixed_in, ffn_gain, expert_ids.T)
+    )(rank, arrived, mixed_in, ffn_gain, select)
     items = lax.all_to_all(outgoing.reshape(eps, pieces, 128), "ep", 0, 0, tiled=True)
 
-    ids, weights, normed_ffn = lax.optimization_barrier(
-        (expert_ids.T, expert_weights.T, normed_ffn)
-    )
-    combine = call(weigh_body, sds((4 * rows, 2 * tps * eps), BF16), [VMEM] * 2)(ids, weights)
-    give, keep, branch = call(
+    ids, weights, gate_line, normed_ffn = lax.optimization_barrier(
+        (expert_ids.T, expert_weights.T, branch_gate, normed_ffn)
+    )
+    combine, branch = call(
+        weigh_body, (sds((4 * rows, 2 * tps * eps), BF16), sds((rows, 128), F32)), [VMEM] * 4
+    )(ids, weights, normed_ffn, gate_line)
+    give, keep = call(
         dense_body,
-        (sds((rows, width // 2), BF16), sds((rows, width // 2), BF16), sds((rows, 128), F32)),
-        [SMEM] + [VMEM] * 5,
-    )(rank, normed_ffn, dense_gate, dense_up, dense_down, branch_gate)
+        (sds((rows, width // 2), BF16), sds((rows, width // 2), BF16)),
+        [SMEM] + [VMEM] * 4,
+    )(rank, normed_ffn, dense_gate, dense_up, dense_down)
     got = lax.ppermute(give, "tp", [(t, t ^ 2) for t in range(tps)])
     give, left = call(
         halve_body, (sds((rows, quarter), BF16), sds((rows, quarter), F32)), [SMEM] + [VMEM] * 2

time: 102 us -> 100 us (0.980)
  blocking collectives: 14.3 us -> 0 us
  waiting for transfers between devices: 26.3 us -> 37.4 us
  starting transfers between devices: 47.6 us -> 50.3 us
    all_to_all x1 -> x0, blocking collectives: 14.3 us -> none  [local(): mixed_in = lax.all_to_all(partial, 'tp', 0, 0, tiled=True)]
    all_to_all x0 -> x1, waiting for transfers between devices: none -> 10.5 us  [local(): mixed_in = lax.all_to_all(partial, 'tp', 0, 0, tiled=True)]
    all_to_all x0 -> x1, starting transfers between devices: none -> 3.33 us  [local(): mixed_in = lax.all_to_all(partial, 'tp', 0, 0, tiled=True)]
  transfers between devices with their start and end apart: 6 -> 7, of which waited for: 5 -> 6; matrix products, arithmetic and copies ran while one was open for 0% -> 0% of each run, Pallas kernels for 4% -> 5%
where the time goes in v2:
time: 100 us; the launch traced here: 99.9 us
  starting transfers between devices  50.3 us (50%)
  waiting for transfers between devices  37.4 us (37%)
  Pallas kernels  11.4 us (11%)
    all_to_all x1, starting transfers between devices, local(): lax.all_to_all(outgoing.reshape(eps, pieces, 128), 'ep', 0, 0, tiled=True)  24.5 us
    all_to_all x1, waiting for transfers between devices, local(): lax.all_to_all(results.reshape(tps * eps, 2, 128), ('tp', 'ep'), 0, 0, ti...  12.2 us
    all_to_all x1, waiting for transfers between devices, local(): mixed_in = lax.all_to_all(partial, 'tp', 0, 0, tiled=True)  10.5 us
    all_to_all x1, starting transfers between devices, local(): lax.all_to_all(results.reshape(tps * eps, 2, 128), ('tp', 'ep'), 0, 0, ti...  8.98 us
    all_to_all x1, waiting for transfers between devices, local(): lax.all_to_all(outgoing.reshape(eps, pieces, 128), 'ep', 0, 0, tiled=True)  8.42 us
    all_to_all x1, starting transfers between devices, local(): arrived = lax.all_to_all(spread, 'tp', 0, 0, tiled=True)  4.84 us
    all_to_all x1, starting transfers between devices, local(): mixed_in = lax.all_to_all(partial, 'tp', 0, 0, tiled=True)  3.33 us
    pallas_call x1, Pallas kernels, local(): call(mixer_body, (pltpu.HBM((tps, rows, width), BF16), sds((rows, inner,...  3.29 us
  transfers between devices with their start and end apart: 7, of which 6 were waited for; matrix products, arithmetic and copies ran while one was open for 0% of the time, Pallas kernels for 5%

profile of v2, /device:TPU:1, one launch (start us, length us, event | category | flops | bytes accessed | tf_op | source)
XLA Modules:
  0.0 99.9 jit_solution(3277605104543736914)
XLA Ops:
  0.6 1.3 %shard_map.308 = bf16[4,16,256]{2,1,0:T(8,128)(2,1)} custom-call(bf16[16,256]{1,0:T(8,128)(2,1)} %tokens.1), custom_call_target="tpu_custom_call" | custom-call | tf_op jit(solution)/shard_map/pallas_call | solution.py:373
  2.0 4.8 %all-to-all-start = ((bf16[4,16,256]{2,1,0:T(8,128)(2,1)}), bf16[4,16,256]{2,1,0:T(8,128)(2,1)S(1)}, u32[]{:S(2)}, u32[]{:S(2)}) async-start(bf16[4,16,256]{2,1,0:T(8,128)(2,1)} %shard_map.308), calls=%async_computation | async-start | bytes 65536 | tf_op jit(solution)/shard_map/all_to_all | solution.py:380
  6.8 0.0 copy-start.6
  6.8 2.2 %shard_map.309 = (f32[8,128]{1,0:T(8,128)S(1)}, bf16[3072,128]{1,0:T(8,128)(2,1)}, bf16[1024,256]{1,0:T(8,128)(2,1)S(1)}, bf16[136,1024]{1,0:T(8,128)(2,1)S(1)},...) custom-call(s32[1]{0:T(128)} %bitcast.refs_0_.rank, ...), custom_call_target="tpu_custom_call" | custom-call | tf_op jit(solution)/shard_map/pallas_call | solution.py:394
  9.1 2.1 %all-to-all-done.arrived = bf16[4,16,256]{2,1,0:T(8,128)(2,1)S(1)} async-done(((bf16[4,16,256]{2,1,0:T(8,128)(2,1)}), bf16[4,16,256]{2,1,0:T(8,128)(2,1)S(1)}, u32[]{:S(2)}, u32[]{:S(2)}) %all-to-all-start) | async-done | bytes 32800 | tf_op jit(solution)/shard_map/all_to_all | solution.py:380
  11.1 0.0 copy-done.6
  11.1 0.0 copy-start.5
  11.1 3.3 %shard_map.310 = (bf16[4,16,1024]{2,1,0:T(8,128)(2,1)}, f32[16,128,64]{2,1,0:T(8,128)}, bf16[3,16,128]{2,1,0:T(8,128)(2,1)}, bf16[3,16,64]{2,1,0:T(8,128)(2,1)}, bf16[3,16,64]{2,1,0:T(8,128)(2,1)}) custom-call(s32[1]{0:T(128)} %bitcast.refs_0_.rank, f32[8,128]{1,0:T(8,128)S(1)} %get-tuple-element.40.lanes, bf16[4,16,256]{2,1,0:T(8,128)(2,1)S(1)} %all-to-all-done.arrived, ...), custom_call_target="tpu_custom_call" | custom-call | tf_op jit(solution)/shard_map/pallas_call | solution.py:429
  14.4 0.0 copy-start.7
  14.4 2.3 %collective-permute-start.1 = (bf16[3072,128]{1,0:T(8,128)(2,1)}, bf16[3072,128]{1,0:T(8,128)(2,1)S(1)}, u32[]{:S(2)}, u32[]{:S(2)}) collective-permute-start(bf16[3072,128]{1,0:T(8,128)(2,1)} %get-tuple-element.62), channel_id=1, source_target_pairs={{0,1},{1,0},{2,3},{3,2},{4,5},{5,4},{6,7},{7,6},{8,9},{9,8},{10,11... | collective-permute-start | bytes 2359304 | tf_op jit(solution)/shard_map/ppermute | solution.py:443
  16.7 0.0 copy-start.9
  16.8 3.3 %all-to-all-start.1 = ((bf16[4,16,1024]{2,1,0:T(8,128)(2,1)}), bf16[4,16,1024]{2,1,0:T(8,128)(2,1)S(1)}, u32[]{:S(2)}, u32[]{:S(2)}) async-start(bf16[4,16,1024]{2,1,0:T(8,128)(2,1)} %get-tuple-element.52), calls=%async_computation.1 | async-start | bytes 262144 | tf_op jit(solution)/shard_map/all_to_all | solution.py:440
  20.1 0.0 copy-done.7
  20.1 0.0 copy-start.4
  20.1 0.5 shard_map.311.select
  20.6 0.0 copy-start.3
  20.6 10.5 %all-to-all-done.1.mixed_in = bf16[4,16,1024]{2,1,0:T(8,128)(2,1)S(1)} async-done(((bf16[4,16,1024]{2,1,0:T(8,128)(2,1)}), bf16[4,16,1024]{2,1,0:T(8,128)(2,1)S(1)}, u32[]{:S(2)}, u32[]{:S(2)}) %all-to-all-start.1) | async-done | bytes 131104 | tf_op jit(solution)/shard_map/all_to_all | solution.py:440
  31.1 0.0 copy-done.9
  31.1 1.1 %shard_map.312 = (bf16[1024,128]{1,0:T(8,128)(2,1)}, bf16[16,1024]{1,0:T(8,128)(2,1)S(1)}, bf16[16,256]{1,0:T(8,128)(2,1)S(1)}) custom-call(s32[1]{0:T(128)} %bitcast.refs_0_.rank, bf16[4,16,256]{2,1,0:T(8,128)(2,1)S(1)} %all-to-all-done.arrived, bf16[4,16,1024]{2,1,0:T(8,128)(2,1)S(1)} %all-to-all-done.1.mixed_in, bf16[1024]{0:T(1024)(128)(2,1)S(1)} %copy-done.9, ...), custom_call_target="tpu_custom_call" | custom-call | tf_op jit(solution)/shard_map/pallas_call | solution.py:445
  32.1 24.5 %all-to-all-start.2 = ((bf16[128,8,128]{2,1,0:T(8,128)(2,1)}), bf16[128,8,128]{2,1,0:T(8,128)(2,1)S(1)}, u32[]{:S(2)}, u32[]{:S(2)}) async-start(bf16[128,8,128]{2,1,0:T(8,128)(2,1)} %bitcast.34), calls=%async_computation.2 | async-start | bytes 524288 | tf_op jit(solution)/shard_map/all_to_all | solution.py:455
  56.6 0.0 copy-done.5
  56.6 0.0 copy-done.4
  56.6 0.0 copy-done.3
  56.6 0.0 copy-start
  56.6 0.0 copy-start.1
  56.6 0.0 copy-start.2
  56.7 0.4 shard_map.313
  57.1 3.1 %collective-permute-start = (bf16[16,512]{1,0:T(8,128)(2,1)S(1)}, bf16[16,512]{1,0:T(8,128)(2,1)S(1)}, u32[]{:S(2)}, u32[]{:S(2)}) collective-permute-start(bf16[16,512]{1,0:T(8,128)(2,1)S(1)} %get-tuple-element.59), channel_id=1, source_target_pairs={{0,2},{1,3},{2,0},{3,1},{4,6},{5,7},{6,4},{7,5},{8,10},{9,11},{10,... | collective-permute-start | bytes 49160 | tf_op jit(solution)/shard_map/ppermute | solution.py:468
  60.2 3.2 %collective-permute-done.got = bf16[16,512]{1,0:T(8,128)(2,1)S(1)} collective-permute-done((bf16[16,512]{1,0:T(8,128)(2,1)S(1)}, bf16[16,512]{1,0:T(8,128)(2,1)S(1)}, u32[]{:S(2)}, u32[]{:S(2)}) %collective-permute-start) | collective-permute-done | bytes 16416 | tf_op jit(solution)/shard_map/ppermute | solution.py:468
  63.4 8.4 %all-to-all-done.2 = bf16[128,8,128]{2,1,0:T(8,128)(2,1)S(1)} async-done(((bf16[128,8,128]{2,1,0:T(8,128)(2,1)}), bf16[128,8,128]{2,1,0:T(8,128)(2,1)S(1)}, u32[]{:S(2)}, u32[]{:S(2)}) %all-to-all-start.2) | async-done | bytes 262176 | tf_op jit(solution)/shard_map/all_to_all | solution.py:455
  71.8 0.0 collective-permute-done.1.other
  71.8 0.0 copy-done
  71.8 0.0 copy-done.1
  71.8 0.0 copy-done.2
  71.8 1.4 %shard_map.315 = bf16[1024,128]{1,0:T(8,128)(2,1)} custom-call(bf16[1024,128]{1,0:T(8,128)(2,1)S(1)} %bitcast.28, bf16[1024,128]{1,0:T(8,128)(2,1)S(1)} %bitcast.23, bf16[1024,128]{1,0:T(8,128)(2,1)S(1)} %bitcast.25, bf16[128,1024]{1,0:T(8,128)(2,1)S(1)} %bitcast.27, bf16[3072,128]{1,0:T(8,128)(2,1)S(1)} %collective-permute-done.1.other), custom_call_target="tpu_custom_call" | custom-call | tf_op jit(solution)/shard_map/pallas_call | solution.py:475
  73.3 0.0 copy-start.8
  73.3 0.0 copy-start.10
  73.3 9.0 %all-to-all-start.3 = ((bf16[512,2,128]{2,1,0:T(2,128)(2,1)}), bf16[512,2,128]{2,1,0:T(2,128)(2,1)S(1)}, u32[]{:S(2)}, u32[]{:S(2)}) async-start(bf16[512,2,128]{2,1,0:T(2,128)(2,1)} %bitcast.33), calls=%async_computation.3 | async-start | bytes 524288 | tf_op jit(solution)/shard_map/all_to_all | solution.py:481
  82.2 3.3 %collective-permute-start.2 = (bf16[16,256]{1,0:T(8,128)(2,1)S(1)}, bf16[16,256]{1,0:T(8,128)(2,1)S(1)}, u32[]{:S(2)}, u32[]{:S(2)}) collective-permute-start(bf16[16,256]{1,0:T(8,128)(2,1)S(1)} %get-tuple-element.68), channel_id=1, source_target_pairs={{0,1},{1,0},{2,3},{3,2},{4,5},{5,4},{6,7},{7,6},{8,9},{9,8},{10,11... | collective-permute-start | bytes 24584 | tf_op jit(solution)/shard_map/ppermute | solution.py:473
  85.5 0.0 copy-done.8
  85.5 0.0 copy-done.10
  85.5 0.4 shard_map.316
  85.9 1.1 %collective-permute-done.2.got = bf16[16,256]{1,0:T(8,128)(2,1)S(1)} collective-permute-done((bf16[16,256]{1,0:T(8,128)(2,1)S(1)}, bf16[16,256]{1,0:T(8,128)(2,1)S(1)}, u32[]{:S(2)}, u32[]{:S(2)}) %collective-permute-start.2) | collective-permute-done | bytes 8224 | tf_op jit(solution)/shard_map/ppermute | solution.py:473
  86.9 12.2 %all-to-all-done.3 = bf16[512,2,128]{2,1,0:T(2,128)(2,1)S(1)} async-done(((bf16[512,2,128]{2,1,0:T(2,128)(2,1)}), bf16[512,2,128]{2,1,0:T(2,128)(2,1)S(1)}, u32[]{:S(2)}, u32[]{:S(2)}) %all-to-all-start.3) | async-done | bytes 262176 | tf_op jit(solution)/shard_map/all_to_all | solution.py:481
  99.1 0.8 shard_map.317
  (1 shorter events, 0.0 us)
Async XLA Ops:
  2.0 9.1 %all-to-all-start = ((bf16[4,16,256]{2,1,0:T(8,128)(2,1)}), bf16[4,16,256]{2,1,0:T(8,128)(2,1)S(1)}, u32[]{:S(2)}, u32[]{:S(2)}) async-start(bf16[4,16,256]{2,1,0:T(8,128)(2,1)} %shard_map.308), calls=%async_computation | async-start | bytes 65536 | tf_op jit(solution)/shard_map/all_to_all | solution.py:380
  6.8 4.3 %copy-start.6 = (bf16[128,1024]{1,0:T(8,128)(2,1)S(1)}, bf16[128,1024]{1,0:T(8,128)(2,1)}, u32[]{:S(2)}) copy-start(bf16[128,1024]{1,0:T(8,128)(2,1)} %proj_out.1) | copy-start | bytes 786436
  11.1 45.5 %copy-start.5 = (bf16[1024,256]{1,0:T(8,128)(2,1)S(1)}, bf16[1024,256]{1,0:T(8,128)(2,1)}, u32[]{:S(2)}) copy-start(bf16[1024,256]{1,0:T(8,128)(2,1)} %down.1) | copy-start | bytes 1572868
  14.4 5.7 %copy-start.7 = (s32[16,6]{0,1:T(8,128)S(1)}, s32[16,6]{0,1:T(8,128)}, u32[]{:S(2)}) copy-start(s32[16,6]{0,1:T(8,128)} %param.49) | copy-start | bytes 1156
  14.4 57.4 %collective-permute-start.1 = (bf16[3072,128]{1,0:T(8,128)(2,1)}, bf16[3072,128]{1,0:T(8,128)(2,1)S(1)}, u32[]{:S(2)}, u32[]{:S(2)}) collective-permute-start(bf16[3072,128]{1,0:T(8,128)(2,1)} %get-tuple-element.62), channel_id=1, source_target_pairs={{0,1},{1,0},{2,3},{3,2},{4,5},{5,4},{6,7},{7,6},{8,9},{9,8},{10,11... | collective-permute-start | bytes 2359304 | tf_op jit(solution)/shard_map/ppermute | solution.py:443
  16.7 14.3 %copy-start.9 = (bf16[1024]{0:T(1024)(128)(2,1)S(1)}, bf16[1024]{0:T(1024)(128)(2,1)}, u32[]{:S(2)}) copy-start(bf16[1024]{0:T(1024)(128)(2,1)} %ffn_gain.1) | copy-start | bytes 6148
  16.8 14.3 %all-to-all-start.1 = ((bf16[4,16,1024]{2,1,0:T(8,128)(2,1)}), bf16[4,16,1024]{2,1,0:T(8,128)(2,1)S(1)}, u32[]{:S(2)}, u32[]{:S(2)}) async-start(bf16[4,16,1024]{2,1,0:T(8,128)(2,1)} %get-tuple-element.52), calls=%async_computation.1 | async-start | bytes 262144 | tf_op jit(solution)/shard_map/all_to_all | solution.py:440
  20.1 36.5 %copy-start.4 = (bf16[1024,256]{1,0:T(8,128)(2,1)S(1)}, bf16[1024,256]{1,0:T(8,128)(2,1)}, u32[]{:S(2)}) copy-start(bf16[1024,256]{1,0:T(8,128)(2,1)} %up.1) | copy-start | bytes 1572868
  20.6 36.0 %copy-start.3 = (bf16[1024,256]{1,0:T(8,128)(2,1)S(1)}, bf16[1024,256]{1,0:T(8,128)(2,1)}, u32[]{:S(2)}) copy-start(bf16[1024,256]{1,0:T(8,128)(2,1)} %gate.1) | copy-start | bytes 1572868
  32.1 39.7 %all-to-all-start.2 = ((bf16[128,8,128]{2,1,0:T(8,128)(2,1)}), bf16[128,8,128]{2,1,0:T(8,128)(2,1)S(1)}, u32[]{:S(2)}, u32[]{:S(2)}) async-start(bf16[128,8,128]{2,1,0:T(8,128)(2,1)} %bitcast.34), calls=%async_computation.2 | async-start | bytes 524288 | tf_op jit(solution)/shard_map/all_to_all | solution.py:455
  56.6 15.2 %copy-start = (bf16[1,1024,128]{2,1,0:T(8,128)(2,1)S(1)}, bf16[1,1024,128]{2,1,0:T(8,128)(2,1)}, u32[]{:S(2)}) copy-start(bf16[1,1024,128]{2,1,0:T(8,128)(2,1)} %param.51) | copy-start | bytes 786436
  56.6 15.2 %copy-start.1 = (bf16[1,1024,128]{2,1,0:T(8,128)(2,1)S(1)}, bf16[1,1024,128]{2,1,0:T(8,128)(2,1)}, u32[]{:S(2)}) copy-start(bf16[1,1024,128]{2,1,0:T(8,128)(2,1)} %param.52) | copy-start | bytes 786436
  56.6 15.2 %copy-start.2 = (bf16[1,128,1024]{2,1,0:T(8,128)(2,1)S(1)}, bf16[1,128,1024]{2,1,0:T(8,128)(2,1)}, u32[]{:S(2)}) copy-start(bf16[1,128,1024]{2,1,0:T(8,128)(2,1)} %param.53) | copy-start | bytes 786436
  57.1 6.3 %collective-permute-start = (bf16[16,512]{1,0:T(8,128)(2,1)S(1)}, bf16[16,512]{1,0:T(8,128)(2,1)S(1)}, u32[]{:S(2)}, u32[]{:S(2)}) collective-permute-start(bf16[16,512]{1,0:T(8,128)(2,1)S(1)} %get-tuple-element.59), channel_id=1, source_target_pairs={{0,2},{1,3},{2,0},{3,1},{4,6},{5,7},{6,4},{7,5},{8,10},{9,11},{10,... | collective-permute-start | bytes 49160 | tf_op jit(solution)/shard_map/ppermute | solution.py:468
  73.3 12.3 %copy-start.8 = (f32[16,6]{0,1:T(8,128)S(1)}, f32[16,6]{0,1:T(8,128)}, u32[]{:S(2)}) copy-start(f32[16,6]{0,1:T(8,128)} %param.50) | copy-start | bytes 1156
  73.3 12.3 %copy-start.10 = (bf16[1024]{0:T(1024)(128)(2,1)S(1)}, bf16[1024]{0:T(1024)(128)(2,1)}, u32[]{:S(2)}) copy-start(bf16[1024]{0:T(1024)(128)(2,1)} %branch_gate) | copy-start | bytes 6148
  73.3 25.9 %all-to-all-start.3 = ((bf16[512,2,128]{2,1,0:T(2,128)(2,1)}), bf16[512,2,128]{2,1,0:T(2,128)(2,1)S(1)}, u32[]{:S(2)}, u32[]{:S(2)}) async-start(bf16[512,2,128]{2,1,0:T(2,128)(2,1)} %bitcast.33), calls=%async_computation.3 | async-start | bytes 524288 | tf_op jit(solution)/shard_map/all_to_all | solution.py:481
  82.2 4.7 %collective-permute-start.2 = (bf16[16,256]{1,0:T(8,128)(2,1)S(1)}, bf16[16,256]{1,0:T(8,128)(2,1)S(1)}, u32[]{:S(2)}, u32[]{:S(2)}) collective-permute-start(bf16[16,256]{1,0:T(8,128)(2,1)S(1)} %get-tuple-element.68), channel_id=1, source_target_pairs={{0,1},{1,0},{2,3},{3,2},{4,5},{5,4},{6,7},{7,6},{8,9},{9,8},{10,11... | collective-permute-start | bytes 24584 | tf_op jit(solution)/shard_map/ppermute | solution.py:473

commit v3 on v2

--- a/solution.py
+++ b/solution.py
@@ -258,7 +258,7 @@
 
 
 def hidden_body(
-    rank, arrived, mixed_in, ffn_gain, select, outgoing, normed_out, hidden_part, folded
+    rank, arrived, mixed_in, ffn_gain, select, outgoing, normed_out, hidden_part, folded, staged, sems
 ):
     count, rows, quarter = arrived.shape
     pieces = folded.shape[0] // rows
@@ -273,11 +273,20 @@
     normed_out[...] = normed_wide.astype(BF16)
     for j in range(pieces):
         folded[pl.ds(j, rows, stride=pieces), :] = normed_wide[:, j * 128 : (j + 1) * 128]
-    outgoing[...] = nn(select[...], folded[...].astype(BF16)).astype(BF16)
-    part = wide[:, 0:quarter]
+    lines = folded[...].astype(BF16)
+    share = outgoing.shape[0] // 4
+    copies = []
+    for q in range(4):
+        part = pl.ds(q * share, share)
+        staged[part, :] = nn(select[part, :], lines).astype(BF16)
+        copies.append(pltpu.make_async_copy(staged.at[part], outgoing.at[part], sems.at[q]))
+        copies[q].start()
+    mine = wide[:, 0:quarter]
     for j in range(1, count):
-        part = jnp.where(rank[0] == j, wide[:, j * quarter : (j + 1) * quarter], part)
-    hidden_part[...] = part.astype(BF16)
+        mine = jnp.where(rank[0] == j, wide[:, j * quarter : (j + 1) * quarter], mine)
+    hidden_part[...] = mine.astype(BF16)
+    for copy in copies:
+        copy.wait()
 
 
 def dense_body(rank, normed_in, gate, up, down, give, keep):
@@ -298,7 +307,7 @@
     left[...] = jnp.where(odd, total[:, quarter:], total[:, 0:quarter])
 
 
-def expert_body(items, gate, up, down, other, out, unfolded, fold):
+def expert_body(items, gate, up, down, other, out, unfolded, fold, staged, sems):
     width, block = gate.shape
     pieces = width // 128
     count = items.shape[0] // pieces
@@ -308,12 +317,21 @@
     )
     act = (silu(nn(x, gate[...])) * nn(x, up[...])).astype(BF16)
     act_other = (silu(nn(x, other[0:width])) * nn(x, other[width : 2 * width])).astype(BF16)
-    total = nn(act, down[...])
-    for j in range(pieces):
-        first = 2 * width + j * block
-        piece = total[:, j * block : (j + 1) * block] + nn(act_other, other[first : first + block])
-        fold[pl.ds(j // 2 * 2 * count + j % 2, count, stride=2), :] = piece
-    out[...] = fold[...].astype(BF16)
+    copies = []
+    for q in range(pieces // 2):
+        at = q * 2 * count
+        total = nn(act, down[:, 2 * q * block : 2 * (q + 1) * block])
+        for h in range(2):
+            first = 2 * width + (2 * q + h) * block
+            piece = nn(act_other, other[first : first + block])
+            piece += total[:, h * block : (h + 1) * block]
+            fold[pl.ds(at + h, count, stride=2), :] = piece
+        staged[at : at + 2 * count] = fold[at : at + 2 * count].astype(BF16)
+        part = pl.ds(at, 2 * count)
+        copies.append(pltpu.make_async_copy(staged.at[part], out.at[part], sems.at[q]))
+        copies[q].start()
+    for copy in copies:
+        copy.wait()
 
 
 def final_body(returned, combine, left, got, branch, hidden_part, out):
@@ -450,7 +468,12 @@
             sds((rows, quarter), BF16),
         ),
         [SMEM] + [VMEM] * 4,
-        [pltpu.VMEM((rows * pieces, 128), F32)],
+        [
+            pltpu.VMEM((rows * pieces, 128), F32),
+            pltpu.VMEM((eps * pieces, 128), BF16),
+            pltpu.SemaphoreType.DMA((4,)),
+        ],
+        (HBM, VMEM, VMEM),
     )(rank, arrived, mixed_in, ffn_gain, select)
     items = lax.all_to_all(outgoing.reshape(eps, pieces, 128), "ep", 0, 0, tiled=True)
 
@@ -476,7 +499,13 @@
         expert_body,
         pltpu.HBM((tps * eps * 2, 128), BF16),
         [VMEM] * 5,
-        [pltpu.VMEM((eps * pieces, 128), F32), pltpu.VMEM((tps * eps * 2, 128), F32)],
+        [
+            pltpu.VMEM((eps * pieces, 128), F32),
+            pltpu.VMEM((tps * eps * 2, 128), F32),
+            pltpu.VMEM((tps * eps * 2, 128), BF16),
+            pltpu.SemaphoreType.DMA((tps,)),
+        ],
+        HBM,
     )(items.reshape(eps * pieces, 128), expert_gate[0], expert_up[0], expert_down[0], other)
     returned = lax.all_to_all(
         results.reshape(tps * eps, 2, 128), ("tp", "ep"), 0, 0, tiled=True

time: 100 us -> 101 us (1.010)
  no operation moved by 1% of the time
where the time goes in v3:
time: 101 us; the launch traced here: 100 us
  starting transfers between devices  50.3 us (50%)
  waiting for transfers between devices  37.4 us (37%)
  Pallas kernels  11.4 us (11%)
    all_to_all x1, starting transfers between devices, local(): lax.all_to_all(outgoing.reshape(eps, pieces, 128), 'ep', 0, 0, tiled=True)  24.5 us
    all_to_all x1, waiting for transfers between devices, local(): lax.all_to_all(results.reshape(tps * eps, 2, 128), ('tp', 'ep'), 0, 0, ti...  12.2 us
    all_to_all x1, waiting for transfers between devices, local(): mixed_in = lax.all_to_all(partial, 'tp', 0, 0, tiled=True)  10.5 us
    all_to_all x1, starting transfers between devices, local(): lax.all_to_all(results.reshape(tps * eps, 2, 128), ('tp', 'ep'), 0, 0, ti...  8.98 us
    all_to_all x1, waiting for transfers between devices, local(): lax.all_to_all(outgoing.reshape(eps, pieces, 128), 'ep', 0, 0, tiled=True)  8.42 us
    all_to_all x1, starting transfers between devices, local(): arrived = lax.all_to_all(spread, 'tp', 0, 0, tiled=True)  4.84 us
    all_to_all x1, starting transfers between devices, local(): mixed_in = lax.all_to_all(partial, 'tp', 0, 0, tiled=True)  3.33 us
    pallas_call x1, Pallas kernels, local(): call(mixer_body, (pltpu.HBM((tps, rows, width), BF16), sds((rows, inner,...  3.29 us
  transfers between devices with their start and end apart: 7, of which 6 were waited for; matrix products, arithmetic and copies ran while one was open for 0% of the time, Pallas kernels for 5%

profile of v3, /device:TPU:1, one launch (start us, length us, event | category | flops | bytes accessed | tf_op | source)
XLA Modules:
  0.0 100.0 jit_solution(7452416229010426556)
XLA Ops:
  0.6 1.3 %shard_map.308 = bf16[4,16,256]{2,1,0:T(8,128)(2,1)} custom-call(bf16[16,256]{1,0:T(8,128)(2,1)} %tokens.1), custom_call_target="tpu_custom_call" | custom-call | tf_op jit(solution)/shard_map/pallas_call | solution.py:391
  2.0 4.8 %all-to-all-start = ((bf16[4,16,256]{2,1,0:T(8,128)(2,1)}), bf16[4,16,256]{2,1,0:T(8,128)(2,1)S(1)}, u32[]{:S(2)}, u32[]{:S(2)}) async-start(bf16[4,16,256]{2,1,0:T(8,128)(2,1)} %shard_map.308), calls=%async_computation | async-start | bytes 65536 | tf_op jit(solution)/shard_map/all_to_all | solution.py:398
  6.8 0.0 copy-start.6
  6.8 2.2 %shard_map.309 = (f32[8,128]{1,0:T(8,128)S(1)}, bf16[3072,128]{1,0:T(8,128)(2,1)}, bf16[1024,256]{1,0:T(8,128)(2,1)S(1)}, bf16[136,1024]{1,0:T(8,128)(2,1)S(1)},...) custom-call(s32[1]{0:T(128)} %bitcast.refs_0_.rank, ...), custom_call_target="tpu_custom_call" | custom-call | tf_op jit(solution)/shard_map/pallas_call | solution.py:412
  9.1 2.1 %all-to-all-done.arrived = bf16[4,16,256]{2,1,0:T(8,128)(2,1)S(1)} async-done(((bf16[4,16,256]{2,1,0:T(8,128)(2,1)}), bf16[4,16,256]{2,1,0:T(8,128)(2,1)S(1)}, u32[]{:S(2)}, u32[]{:S(2)}) %all-to-all-start) | async-done | bytes 32800 | tf_op jit(solution)/shard_map/all_to_all | solution.py:398
  11.1 0.0 copy-done.6
  11.1 0.0 copy-start.5
  11.1 3.3 %shard_map.310 = (bf16[4,16,1024]{2,1,0:T(8,128)(2,1)}, f32[16,128,64]{2,1,0:T(8,128)}, bf16[3,16,128]{2,1,0:T(8,128)(2,1)}, bf16[3,16,64]{2,1,0:T(8,128)(2,1)}, bf16[3,16,64]{2,1,0:T(8,128)(2,1)}) custom-call(s32[1]{0:T(128)} %bitcast.refs_0_.rank, f32[8,128]{1,0:T(8,128)S(1)} %get-tuple-element.40.lanes, bf16[4,16,256]{2,1,0:T(8,128)(2,1)S(1)} %all-to-all-done.arrived, ...), custom_call_target="tpu_custom_call" | custom-call | tf_op jit(solution)/shard_map/pallas_call | solution.py:447
  14.4 0.0 copy-start.7
  14.4 2.3 %collective-permute-start.1 = (bf16[3072,128]{1,0:T(8,128)(2,1)}, bf16[3072,128]{1,0:T(8,128)(2,1)S(1)}, u32[]{:S(2)}, u32[]{:S(2)}) collective-permute-start(bf16[3072,128]{1,0:T(8,128)(2,1)} %get-tuple-element.62), channel_id=1, source_target_pairs={{0,1},{1,0},{2,3},{3,2},{4,5},{5,4},{6,7},{7,6},{8,9},{9,8},{10,11... | collective-permute-start | bytes 2359304 | tf_op jit(solution)/shard_map/ppermute | solution.py:461
  16.7 0.0 copy-start.9
  16.8 3.3 %all-to-all-start.1 = ((bf16[4,16,1024]{2,1,0:T(8,128)(2,1)}), bf16[4,16,1024]{2,1,0:T(8,128)(2,1)S(1)}, u32[]{:S(2)}, u32[]{:S(2)}) async-start(bf16[4,16,1024]{2,1,0:T(8,128)(2,1)} %get-tuple-element.52), calls=%async_computation.1 | async-start | bytes 262144 | tf_op jit(solution)/shard_map/all_to_all | solution.py:458
  20.1 0.0 copy-done.7
  20.1 0.0 copy-start.4
  20.1 0.5 shard_map.311.select
  20.6 0.0 copy-start.3
  20.6 10.5 %all-to-all-done.1.mixed_in = bf16[4,16,1024]{2,1,0:T(8,128)(2,1)S(1)} async-done(((bf16[4,16,1024]{2,1,0:T(8,128)(2,1)}), bf16[4,16,1024]{2,1,0:T(8,128)(2,1)S(1)}, u32[]{:S(2)}, u32[]{:S(2)}) %all-to-all-start.1) | async-done | bytes 131104 | tf_op jit(solution)/shard_map/all_to_all | solution.py:458
  31.1 0.0 copy-done.9
  31.1 1.0 %shard_map.312 = (bf16[1024,128]{1,0:T(8,128)(2,1)}, bf16[16,1024]{1,0:T(8,128)(2,1)S(1)}, bf16[16,256]{1,0:T(8,128)(2,1)S(1)}) custom-call(s32[1]{0:T(128)} %bitcast.refs_0_.rank, bf16[4,16,256]{2,1,0:T(8,128)(2,1)S(1)} %all-to-all-done.arrived, bf16[4,16,1024]{2,1,0:T(8,128)(2,1)S(1)} %all-to-all-done.1.mixed_in, bf16[1024]{0:T(1024)(128)(2,1)S(1)} %copy-done.9, ...), custom_call_target="tpu_custom_call" | custom-call | tf_op jit(solution)/shard_map/pallas_call | solution.py:463
  32.1 24.5 %all-to-all-start.2 = ((bf16[128,8,128]{2,1,0:T(8,128)(2,1)}), bf16[128,8,128]{2,1,0:T(8,128)(2,1)S(1)}, u32[]{:S(2)}, u32[]{:S(2)}) async-start(bf16[128,8,128]{2,1,0:T(8,128)(2,1)} %bitcast.34), calls=%async_computation.2 | async-start | bytes 524288 | tf_op jit(solution)/shard_map/all_to_all | solution.py:478
  56.6 0.0 copy-done.5
  56.6 0.0 copy-done.4
  56.6 0.0 copy-done.3
  56.6 0.0 copy-start
  56.6 0.0 copy-start.1
  56.7 0.0 copy-start.2
  56.7 0.4 shard_map.313
  57.1 3.1 %collective-permute-start = (bf16[16,512]{1,0:T(8,128)(2,1)S(1)}, bf16[16,512]{1,0:T(8,128)(2,1)S(1)}, u32[]{:S(2)}, u32[]{:S(2)}) collective-permute-start(bf16[16,512]{1,0:T(8,128)(2,1)S(1)} %get-tuple-element.59), channel_id=1, source_target_pairs={{0,2},{1,3},{2,0},{3,1},{4,6},{5,7},{6,4},{7,5},{8,10},{9,11},{10,... | collective-permute-start | bytes 49160 | tf_op jit(solution)/shard_map/ppermute | solution.py:491
  60.2 3.2 %collective-permute-done.got = bf16[16,512]{1,0:T(8,128)(2,1)S(1)} collective-permute-done((bf16[16,512]{1,0:T(8,128)(2,1)S(1)}, bf16[16,512]{1,0:T(8,128)(2,1)S(1)}, u32[]{:S(2)}, u32[]{:S(2)}) %collective-permute-start) | collective-permute-done | bytes 16416 | tf_op jit(solution)/shard_map/ppermute | solution.py:491
  63.4 8.4 %all-to-all-done.2 = bf16[128,8,128]{2,1,0:T(8,128)(2,1)S(1)} async-done(((bf16[128,8,128]{2,1,0:T(8,128)(2,1)}), bf16[128,8,128]{2,1,0:T(8,128)(2,1)S(1)}, u32[]{:S(2)}, u32[]{:S(2)}) %all-to-all-start.2) | async-done | bytes 262176 | tf_op jit(solution)/shard_map/all_to_all | solution.py:478
  71.8 0.0 collective-permute-done.1.other
  71.8 0.0 copy-done
  71.8 0.0 copy-done.1
  71.8 0.0 copy-done.2
  71.9 1.4 %shard_map.315 = bf16[1024,128]{1,0:T(8,128)(2,1)} custom-call(bf16[1024,128]{1,0:T(8,128)(2,1)S(1)} %bitcast.28, bf16[1024,128]{1,0:T(8,128)(2,1)S(1)} %bitcast.23, bf16[1024,128]{1,0:T(8,128)(2,1)S(1)} %bitcast.25, bf16[128,1024]{1,0:T(8,128)(2,1)S(1)} %bitcast.27, bf16[3072,128]{1,0:T(8,128)(2,1)S(1)} %collective-permute-done.1.other), custom_call_target="tpu_custom_call" | custom-call | tf_op jit(solution)/shard_map/pallas_call | solution.py:498
  73.3 0.0 copy-start.8
  73.3 0.0 copy-start.10
  73.3 9.0 %all-to-all-start.3 = ((bf16[512,2,128]{2,1,0:T(2,128)(2,1)}), bf16[512,2,128]{2,1,0:T(2,128)(2,1)S(1)}, u32[]{:S(2)}, u32[]{:S(2)}) async-start(bf16[512,2,128]{2,1,0:T(2,128)(2,1)} %bitcast.33), calls=%async_computation.3 | async-start | bytes 524288 | tf_op jit(solution)/shard_map/all_to_all | solution.py:510
  82.3 3.3 %collective-permute-start.2 = (bf16[16,256]{1,0:T(8,128)(2,1)S(1)}, bf16[16,256]{1,0:T(8,128)(2,1)S(1)}, u32[]{:S(2)}, u32[]{:S(2)}) collective-permute-start(bf16[16,256]{1,0:T(8,128)(2,1)S(1)} %get-tuple-element.68), channel_id=1, source_target_pairs={{0,1},{1,0},{2,3},{3,2},{4,5},{5,4},{6,7},{7,6},{8,9},{9,8},{10,11... | collective-permute-start | bytes 24584 | tf_op jit(solution)/shard_map/ppermute | solution.py:496
  85.6 0.0 copy-done.8
  85.6 0.0 copy-done.10
  85.6 0.4 shard_map.316
  86.0 1.1 %collective-permute-done.2.got = bf16[16,256]{1,0:T(8,128)(2,1)S(1)} collective-permute-done((bf16[16,256]{1,0:T(8,128)(2,1)S(1)}, bf16[16,256]{1,0:T(8,128)(2,1)S(1)}, u32[]{:S(2)}, u32[]{:S(2)}) %collective-permute-start.2) | collective-permute-done | bytes 8224 | tf_op jit(solution)/shard_map/ppermute | solution.py:496
  87.0 12.2 %all-to-all-done.3 = bf16[512,2,128]{2,1,0:T(2,128)(2,1)S(1)} async-done(((bf16[512,2,128]{2,1,0:T(2,128)(2,1)}), bf16[512,2,128]{2,1,0:T(2,128)(2,1)S(1)}, u32[]{:S(2)}, u32[]{:S(2)}) %all-to-all-start.3) | async-done | bytes 262176 | tf_op jit(solution)/shard_map/all_to_all | solution.py:510
  99.2 0.8 shard_map.317
  (1 shorter events, 0.0 us)
Async XLA Ops:
  2.0 9.1 %all-to-all-start = ((bf16[4,16,256]{2,1,0:T(8,128)(2,1)}), bf16[4,16,256]{2,1,0:T(8,128)(2,1)S(1)}, u32[]{:S(2)}, u32[]{:S(2)}) async-start(bf16[4,16,256]{2,1,0:T(8,128)(2,1)} %shard_map.308), calls=%async_computation | async-start | bytes 65536 | tf_op jit(solution)/shard_map/all_to_all | solution.py:398
  6.8 4.3 %copy-start.6 = (bf16[128,1024]{1,0:T(8,128)(2,1)S(1)}, bf16[128,1024]{1,0:T(8,128)(2,1)}, u32[]{:S(2)}) copy-start(bf16[128,1024]{1,0:T(8,128)(2,1)} %proj_out.1) | copy-start | bytes 786436
  11.1 45.5 %copy-start.5 = (bf16[1024,256]{1,0:T(8,128)(2,1)S(1)}, bf16[1024,256]{1,0:T(8,128)(2,1)}, u32[]{:S(2)}) copy-start(bf16[1024,256]{1,0:T(8,128)(2,1)} %down.1) | copy-start | bytes 1572868
  14.4 5.7 %copy-start.7 = (s32[16,6]{0,1:T(8,128)S(1)}, s32[16,6]{0,1:T(8,128)}, u32[]{:S(2)}) copy-start(s32[16,6]{0,1:T(8,128)} %param.49) | copy-start | bytes 1156
  14.4 57.4 %collective-permute-start.1 = (bf16[3072,128]{1,0:T(8,128)(2,1)}, bf16[3072,128]{1,0:T(8,128)(2,1)S(1)}, u32[]{:S(2)}, u32[]{:S(2)}) collective-permute-start(bf16[3072,128]{1,0:T(8,128)(2,1)} %get-tuple-element.62), channel_id=1, source_target_pairs={{0,1},{1,0},{2,3},{3,2},{4,5},{5,4},{6,7},{7,6},{8,9},{9,8},{10,11... | collective-permute-start | bytes 2359304 | tf_op jit(solution)/shard_map/ppermute | solution.py:461
  16.7 14.3 %copy-start.9 = (bf16[1024]{0:T(1024)(128)(2,1)S(1)}, bf16[1024]{0:T(1024)(128)(2,1)}, u32[]{:S(2)}) copy-start(bf16[1024]{0:T(1024)(128)(2,1)} %ffn_gain.1) | copy-start | bytes 6148
  16.8 14.3 %all-to-all-start.1 = ((bf16[4,16,1024]{2,1,0:T(8,128)(2,1)}), bf16[4,16,1024]{2,1,0:T(8,128)(2,1)S(1)}, u32[]{:S(2)}, u32[]{:S(2)}) async-start(bf16[4,16,1024]{2,1,0:T(8,128)(2,1)} %get-tuple-element.52), calls=%async_computation.1 | async-start | bytes 262144 | tf_op jit(solution)/shard_map/all_to_all | solution.py:458
  20.1 36.5 %copy-start.4 = (bf16[1024,256]{1,0:T(8,128)(2,1)S(1)}, bf16[1024,256]{1,0:T(8,128)(2,1)}, u32[]{:S(2)}) copy-start(bf16[1024,256]{1,0:T(8,128)(2,1)} %up.1) | copy-start | bytes 1572868
  20.6 36.0 %copy-start.3 = (bf16[1024,256]{1,0:T(8,128)(2,1)S(1)}, bf16[1024,256]{1,0:T(8,128)(2,1)}, u32[]{:S(2)}) copy-start(bf16[1024,256]{1,0:T(8,128)(2,1)} %gate.1) | copy-start | bytes 1572868
  32.1 39.7 %all-to-all-start.2 = ((bf16[128,8,128]{2,1,0:T(8,128)(2,1)}), bf16[128,8,128]{2,1,0:T(8,128)(2,1)S(1)}, u32[]{:S(2)}, u32[]{:S(2)}) async-start(bf16[128,8,128]{2,1,0:T(8,128)(2,1)} %bitcast.34), calls=%async_computation.2 | async-start | bytes 524288 | tf_op jit(solution)/shard_map/all_to_all | solution.py:478
  56.6 15.2 %copy-start = (bf16[1,1024,128]{2,1,0:T(8,128)(2,1)S(1)}, bf16[1,1024,128]{2,1,0:T(8,128)(2,1)}, u32[]{:S(2)}) copy-start(bf16[1,1024,128]{2,1,0:T(8,128)(2,1)} %param.51) | copy-start | bytes 786436
  56.6 15.2 %copy-start.1 = (bf16[1,1024,128]{2,1,0:T(8,128)(2,1)S(1)}, bf16[1,1024,128]{2,1,0:T(8,128)(2,1)}, u32[]{:S(2)}) copy-start(bf16[1,1024,128]{2,1,0:T(8,128)(2,1)} %param.52) | copy-start | bytes 786436
  56.7 15.2 %copy-start.2 = (bf16[1,128,1024]{2,1,0:T(8,128)(2,1)S(1)}, bf16[1,128,1024]{2,1,0:T(8,128)(2,1)}, u32[]{:S(2)}) copy-start(bf16[1,128,1024]{2,1,0:T(8,128)(2,1)} %param.53) | copy-start | bytes 786436
  57.1 6.3 %collective-permute-start = (bf16[16,512]{1,0:T(8,128)(2,1)S(1)}, bf16[16,512]{1,0:T(8,128)(2,1)S(1)}, u32[]{:S(2)}, u32[]{:S(2)}) collective-permute-start(bf16[16,512]{1,0:T(8,128)(2,1)S(1)} %get-tuple-element.59), channel_id=1, source_target_pairs={{0,2},{1,3},{2,0},{3,1},{4,6},{5,7},{6,4},{7,5},{8,10},{9,11},{10,... | collective-permute-start | bytes 49160 | tf_op jit(solution)/shard_map/ppermute | solution.py:491
  73.3 12.3 %copy-start.8 = (f32[16,6]{0,1:T(8,128)S(1)}, f32[16,6]{0,1:T(8,128)}, u32[]{:S(2)}) copy-start(f32[16,6]{0,1:T(8,128)} %param.50) | copy-start | bytes 1156
  73.3 12.3 %copy-start.10 = (bf16[1024]{0:T(1024)(128)(2,1)S(1)}, bf16[1024]{0:T(1024)(128)(2,1)}, u32[]{:S(2)}) copy-start(bf16[1024]{0:T(1024)(128)(2,1)} %branch_gate) | copy-start | bytes 6148
  73.3 25.9 %all-to-all-start.3 = ((bf16[512,2,128]{2,1,0:T(2,128)(2,1)}), bf16[512,2,128]{2,1,0:T(2,128)(2,1)S(1)}, u32[]{:S(2)}, u32[]{:S(2)}) async-start(bf16[512,2,128]{2,1,0:T(2,128)(2,1)} %bitcast.33), calls=%async_computation.3 | async-start | bytes 524288 | tf_op jit(solution)/shard_map/all_to_all | solution.py:510
  82.3 4.7 %collective-permute-start.2 = (bf16[16,256]{1,0:T(8,128)(2,1)S(1)}, bf16[16,256]{1,0:T(8,128)(2,1)S(1)}, u32[]{:S(2)}, u32[]{:S(2)}) collective-permute-start(bf16[16,256]{1,0:T(8,128)(2,1)S(1)} %get-tuple-element.68), channel_id=1, source_target_pairs={{0,1},{1,0},{2,3},{3,2},{4,5},{5,4},{6,7},{7,6},{8,9},{9,8},{10,11... | collective-permute-start | bytes 24584 | tf_op jit(solution)/shard_map/ppermute | solution.py:496
